TPU v7x, 32 devices: a whole 2x2x4 slice. The times are simulated.
32 devices in a mesh: ep: 16 (over z, y, x), tp: 2 (over core).
Axes of the slice: x: 2, y: 2, z: 4, core: 2. Of those that a mesh axis runs over, the one named last changes fastest.
Arguments:
- inputs: bfloat16 [256, 2048], P('ep'), may hold values from -6 to 6
- positions: int32 [256], P('ep'), may hold values from 1024 to 8191
- ret_state: float32 [256, 12, 128, 128], P('ep', 'tp'), may hold values from -4 to 4
- norm_mix: bfloat16 [2048], replicated, may hold values from 0.099609375 to 1.8984375
- w_query: bfloat16 [2048, 1536], P('ep', 'tp'), may hold values from -0.1875 to 0.1875
- w_key: bfloat16 [2048, 1536], P('ep', 'tp'), may hold values from -0.1875 to 0.1875
- w_value: bfloat16 [2048, 1536], P('ep', 'tp'), may hold values from -0.1875 to 0.1875
- w_gate_in: bfloat16 [2048, 1536], P('ep', 'tp'), may hold values from -0.1875 to 0.1875
- head_gain: bfloat16 [1536], P('tp'), may hold values from 0.099609375 to 1.8984375
- w_out: bfloat16 [1536, 2048], P('tp', 'ep'), may hold values from -0.15625 to 0.15625
- norm_ffn: bfloat16 [2048], replicated, may hold values from 0.099609375 to 1.8984375
- route_ids: int32 [256, 4], P('ep'), may hold values from 0 to 15, all different within a row; in each aligned block of 16 rows (0 to 15, 16 to 31, ...) at most 8 rows name the same one
- route_weight: bfloat16 [256, 4], P('ep'), may hold values from 0.19921875 to 1
- exp_gate: bfloat16 [16, 2048, 1024], P('ep', None, 'tp'), may hold values from -0.125 to 0.125
- exp_up: bfloat16 [16, 2048, 1024], P('ep', None, 'tp'), may hold values from -0.125 to 0.125
- exp_down: bfloat16 [16, 1024, 2048], P('ep', 'tp'), may hold values from -0.1875 to 0.1875
- dense_gate: bfloat16 [2048, 4096], P(None, ('ep', 'tp')), may hold values from -0.125 to 0.125
- dense_up: bfloat16 [2048, 4096], P(None, ('ep', 'tp')), may hold values from -0.125 to 0.125
- dense_down: bfloat16 [4096, 2048], P(('ep', 'tp')), may hold values from -0.1875 to 0.1875
- branch_gate: bfloat16 [2048], replicated, may hold values from -0.125 to 0.125
Outputs:
- layer_out: bfloat16 [256, 2048], P('ep')
- new_state: float32 [256, 12, 128, 128], P('ep', 'tp')
Inputs may be any that keep to these rules, and one draw needn't show every extreme that they name: `route_ids`: each row names 4 different experts. Among the rows of one index of ep no expert is named more than 8 times, a bound that some block reaches.
All inputs are finite; a program needn't handle non-finite values.
Results may differ from a plain program's by a relative error of at most 0.015.
Values may be sent and summed in bfloat16 or wider, within the bound.
A program may use at most 128 MiB of HBM per device.

v0:
```python
import functools

import jax
import jax.numpy as jnp
from jax import lax
from jax.experimental import pallas as pl
from jax.experimental.pallas import tpu as pltpu
from jax.sharding import PartitionSpec as P

HEADS = 12
EPS = 1e-06
MESH = pl.DeviceIdType.MESH
LANES = 128
F32 = jnp.float32
BF16 = jnp.bfloat16
VMEM_LIMIT = 60 * 1024 * 1024


def rotary_angles(positions, head_dim):
    halfway = head_dim // 2
    frequency = 10000.0 ** (-jnp.arange(halfway, dtype=jnp.float32) * 2.0 / head_dim)
    return positions.astype(jnp.float32)[:, None] * frequency[None, :]


def log_decay(head_count):
    spread = jnp.arange(head_count, dtype=jnp.float32) * (5.0 / max(head_count - 1, 1))
    return jnp.log1p(-(2.0 ** (-5.0 - spread)))


def normalize(values, gain):
    scaled = values * lax.rsqrt(jnp.mean(values * values, axis=-1, keepdims=True) + EPS)
    return (scaled * gain.astype(F32)).astype(BF16)


def greet(n, me, tp, partner=None):
    barrier = pltpu.get_barrier_semaphore()

    @pl.loop(1, n)
    def _(k):
        pl.semaphore_signal(
            barrier, inc=1, device_id=(lax.rem(me + k, n), tp), device_id_type=MESH
        )

    if partner is not None:
        pl.semaphore_signal(barrier, inc=1, device_id=(me, partner), device_id_type=MESH)
    pl.semaphore_wait(barrier, n - 1 + (partner is not None))


def to_peer(src, dst, send, recv, k, ep, tp):
    return pltpu.make_async_remote_copy(
        src_ref=src,
        dst_ref=dst,
        send_sem=send.at[k],
        recv_sem=recv.at[k],
        device_id=(ep, tp),
        device_id_type=MESH,
    )


def scatter_start(n, me, tp, src, dst, send, recv):
    @pl.loop(1, n)
    def _(k):
        peer = lax.rem(me + k, n)
        to_peer(src.at[peer], dst.at[me], send, recv, k, peer, tp).start()


def scatter_wait(n, me, tp, src, dst, send, recv):
    @pl.loop(1, n)
    def _(k):
        peer = lax.rem(me + k, n)
        came = lax.rem(me + n - k, n)
        copy = to_peer(src.at[peer], dst.at[came], send, recv, k, peer, tp)
        copy.wait_send()
        copy.wait_recv()


def project_kernel(
    n, x_ref, gain_ref, ids_ref, weight_ref, wq, wk, wv, wg, out_ref, share_out,
    blocks, columns, parts, plane, reduced, landed, share_ref, shares,
    send, recv, plane_send, plane_recv, line_send, line_recv,
):
    me, tp = lax.axis_index("ep"), lax.axis_index("tp")
    seqs, width = x_ref.shape
    block, local = width // n, wq.shape[1]
    outer, inner = parts.shape[2], parts.shape[1]
    along, inside = me // inner, lax.rem(me, inner)
    normed = normalize(x_ref[...].astype(F32), gain_ref[...])
    for j in range(n):
        blocks[j] = normed[:, j * block : (j + 1) * block]
    greet(n, me, tp)
    sems = lambda i: (send.at[i], recv.at[i])
    scatter_start(n, me, tp, blocks, columns, *sems(0))
    columns[me] = blocks[me]
    widened = weight_ref[...].astype(F32)
    part = widened / jnp.sum(widened, axis=-1, keepdims=True)
    for j in range(n):
        mine = jnp.sum(jnp.where(ids_ref[...] == j, part, 0.0), axis=-1, keepdims=True)
        share_ref[j] = jnp.broadcast_to(mine, (seqs, LANES))
    scatter_start(n, me, tp, share_ref, shares, *sems(1))
    shares[me] = share_ref[me]
    scatter_wait(n, me, tp, blocks, columns, *sems(0))
    rows = columns[...].reshape(n * seqs, block)

    def in_plane(i, k, source):
        peer = lax.rem(inside + k, inner)
        return to_peer(
            parts.at[i, peer], plane.at[i, source], plane_send.at[i], plane_recv.at[i], k,
            me - inside + peer, tp,
        )

    def in_line(i, k, source):
        peer = lax.rem(along + k, outer)
        return to_peer(
            reduced.at[i, peer], landed.at[i, source], line_send.at[i], line_recv.at[i], k,
            peer * inner + inside, tp,
        )

    span = inner * seqs
    for i, w in enumerate((wq, wk, wv, wg)):
        product = jnp.dot(rows, w[...], preferred_element_type=F32).astype(BF16)
        for z in range(outer):
            parts[i, :, z] = product[z * span : (z + 1) * span].reshape(inner, seqs, local)

        @pl.loop(1, inner)
        def _(k):
            in_plane(i, k, inside).start()

        plane[i, inside] = parts[i, inside]

    for i in range(4):

        @pl.loop(1, inner)
        def _(k):
            copy = in_plane(i, k, lax.rem(inside + inner - k, inner))
            copy.wait_send()
            copy.wait_recv()

        for z in range(outer):
            total = lax.fori_loop(
                0,
                inner,
                lambda j, acc: acc + plane[i, j, z].astype(F32),
                jnp.zeros((seqs, local), F32),
            )
            reduced[i, z] = total.astype(BF16)

        @pl.loop(1, outer)
        def _(k):
            in_line(i, k, along).start()

        landed[i, along] = reduced[i, along]

    scatter_wait(n, me, tp, share_ref, shares, *sems(1))
    share_out[...] = shares[...]
    for i in range(4):

        @pl.loop(1, outer)
        def _(k):
            copy = in_line(i, k, lax.rem(along + outer - k, outer))
            copy.wait_send()
            copy.wait_recv()

        total = lax.fori_loop(
            0,
            outer,
            lambda j, acc: acc + landed[i, j].astype(F32),
            jnp.zeros((seqs, local), F32),
        )
        out_ref[:, i * local : (i + 1) * local] = total.astype(BF16)


def project(n, x, gain, ids, weight, weights):
    seqs, width = x.shape
    local = weights[0].shape[1]
    outer = 4 if n % 4 == 0 else 1
    inner = n // outer
    vmem = pl.BlockSpec(memory_space=pltpu.VMEM)
    sem = pltpu.SemaphoreType.DMA
    return pl.pallas_call(
        functools.partial(project_kernel, n),
        out_shape=(
            jax.ShapeDtypeStruct((seqs, 4 * local), BF16),
            jax.ShapeDtypeStruct((n, seqs, LANES), F32),
        ),
        in_specs=[vmem] * 8,
        out_specs=(vmem, vmem),
        scratch_shapes=[
            pltpu.VMEM((n, seqs, width // n), BF16),
            pltpu.VMEM((n, seqs, width // n), BF16),
            pltpu.VMEM((4, inner, outer, seqs, local), BF16),
            pltpu.VMEM((4, inner, outer, seqs, local), BF16),
            pltpu.VMEM((4, outer, seqs, local), BF16),
            pltpu.VMEM((4, outer, seqs, local), BF16),
            pltpu.VMEM((n, seqs, LANES), F32),
            pltpu.VMEM((n, seqs, LANES), F32),
            sem((2, n)),
            sem((2, n)),
            sem((4, inner)),
            sem((4, inner)),
            sem((4, outer)),
            sem((4, outer)),
        ],
        compiler_params=pltpu.CompilerParams(
            collective_id=0, has_side_effects=True, vmem_limit_bytes=VMEM_LIMIT
        ),
    )(x, gain, ids, weight, *weights)


def retain_kernel(
    gamma_ref, q_ref, k_ref, v_ref, g_ref, gain_ref, cos_ref, sin_ref, state_ref,
    new_ref, out_ref, readout,
):
    seqs, dim = q_ref.shape
    gamma = gamma_ref[pl.program_id(0)]
    cos, sin = cos_ref[...], sin_ref[...]

    def rotated(ref):
        val = ref[...].astype(F32)
        return val * cos + pltpu.roll(val, dim // 2, 1) * sin

    query = rotated(q_ref).T
    key = (rotated(k_ref) * dim ** (-0.5)).T
    value = v_ref[...].astype(F32)
    for s in range(seqs):
        new = gamma * state_ref[s, 0] + key[:, s : s + 1] * value[s : s + 1, :]
        new_ref[s, 0] = new
        readout[s : s + 1, :] = jnp.sum(new * query[:, s : s + 1], axis=0, keepdims=True)
    read = readout[...]
    centred = read - jnp.mean(read, axis=-1, keepdims=True)
    normed = centred * lax.rsqrt(jnp.mean(centred * centred, axis=-1, keepdims=True) + EPS)
    gate = g_ref[...].astype(F32)
    out_ref[...] = (
        normed * gain_ref[...].astype(F32) * (gate * jax.nn.sigmoid(gate))
    ).astype(BF16)


def retain(gamma, joined, gain, cos, sin, state):
    seqs, heads, dim = state.shape[:3]
    piece = lambda i: pl.BlockSpec((seqs, dim), lambda h, i=i: (0, i * heads + h))
    whole = pl.BlockSpec((seqs, dim), lambda h: (0, 0))
    held = pl.BlockSpec((seqs, 1, dim, dim), lambda h: (0, h, 0, 0))
    return pl.pallas_call(
        retain_kernel,
        grid=(heads,),
        out_shape=(
            jax.ShapeDtypeStruct(state.shape, F32),
            jax.ShapeDtypeStruct((seqs, heads * dim), BF16),
        ),
        in_specs=[
            pl.BlockSpec(memory_space=pltpu.SMEM),
            piece(0), piece(1), piece(2), piece(3),
            pl.BlockSpec((1, dim), lambda h: (0, h)),
            whole, whole, held,
        ],
        out_specs=(held, pl.BlockSpec((seqs, dim), lambda h: (0, h))),
        scratch_shapes=[pltpu.VMEM((seqs, dim), F32)],
        compiler_params=pltpu.CompilerParams(vmem_limit_bytes=VMEM_LIMIT),
    )(gamma, joined, joined, joined, joined, gain, cos, sin, state)


def mix_kernel(
    n, x_ref, ret_ref, wout_ref, gain_ref, share_ref, open_w, eg_hbm, eu_hbm, ed_hbm,
    dg_hbm, du_hbm, dd_hbm, out_ref,
    heads, cols, cols_in, cols_sum, mixed, mixed_row, half_out, gathered, eg, eu, ed, dg, du, dd,
    hidden, dense_hidden, opening, other, other_in, own, summed, landed, final, final_in,
    load, send, recv, pair_send, pair_recv, relay_send, relay_recv,
):
    me, tp = lax.axis_index("ep"), lax.axis_index("tp")
    mate = 1 - tp
    seqs, width = x_ref.shape
    block, half = width // n, width // 2
    tokens = n * seqs
    loads = [
        pltpu.make_async_copy(src, dst, load.at[i])
        for i, (src, dst) in enumerate(
            ((eg_hbm.at[0], eg), (eu_hbm.at[0], eu), (dg_hbm, dg), (du_hbm, du),
             (ed_hbm.at[0], ed), (dd_hbm, dd))
        )
    ]
    for copy in loads:
        copy.start()
    greet(n, me, tp, mate)
    sems = lambda i: (send.at[i], recv.at[i])
    pair = lambda src, dst, i: to_peer(src, dst, pair_send, pair_recv, i, me, mate)

    @pl.loop(1, n)
    def _(k):
        peer = lax.rem(me + k, n)
        to_peer(ret_ref, heads.at[me], *sems(0), k, peer, tp).start()

    heads[me] = ret_ref[...]

    @pl.loop(1, n)
    def _(k):
        came = lax.rem(me + n - k, n)
        copy = to_peer(ret_ref, heads.at[came], *sems(0), k, lax.rem(me + k, n), tp)
        copy.wait_send()
        copy.wait_recv()

    part = jnp.dot(
        heads[...].reshape(tokens, ret_ref.shape[1]), wout_ref[...], preferred_element_type=F32
    )
    cols[...] = part.astype(BF16).reshape(n, seqs, block)
    swap = pair(cols, cols_in, 0)
    swap.start()
    swap.wait()
    cols_sum[...] = (cols[...].astype(F32) + cols_in[...].astype(F32)).astype(BF16)
    scatter_start(n, me, tp, cols_sum, mixed, *sems(1))
    mixed[me] = cols_sum[me]
    scatter_wait(n, me, tp, cols_sum, mixed, *sems(1))
    for j in range(n):
        mixed_row[:, j * block : (j + 1) * block] = mixed[j].astype(F32)
    residual = (x_ref[...].astype(F32) + mixed_row[...]).astype(BF16)
    mixed_row[...] = residual.astype(F32)
    normed = normalize(residual.astype(F32), gain_ref[...])
    for c in range(2):
        half_out[c] = normed[:, c * half : (c + 1) * half]

    @pl.loop(1, n)
    def _(k):
        peer = lax.rem(me + k, n)
        to_peer(half_out.at[tp], gathered.at[tp, me], *sems(2), k, peer, tp).start()

    for c in range(2):
        gathered[c, me] = half_out[c]

    @pl.loop(1, n)
    def _(k):
        came = lax.rem(me + n - k, n)
        copy = to_peer(
            half_out.at[tp], gathered.at[tp, came], *sems(2), k, lax.rem(me + k, n), tp
        )
        copy.wait_send()
        copy.wait_recv()
        to_peer(
            gathered.at[tp, came], gathered.at[tp, came], relay_send, relay_recv, k, me, mate
        ).start()

    for copy in loads:
        copy.wait()

    @pl.loop(1, n)
    def _(k):
        came = lax.rem(me + n - k, n)
        relay = to_peer(
            gathered.at[tp, came], gathered.at[mate, came], relay_send, relay_recv, k, me, mate
        )
        relay.wait_send()
        relay.wait_recv()

    def features(w, at):
        left = gathered[0].reshape(tokens, half)
        right = gathered[1].reshape(tokens, half)
        return jnp.dot(left, w[:half, at], preferred_element_type=F32) + jnp.dot(
            right, w[half:, at], preferred_element_type=F32
        )

    tile = min(256, eg.shape[1])

    @pl.loop(0, eg.shape[1] // tile)
    def _(j):
        at = pl.ds(pl.multiple_of(j * tile, tile), tile)
        gate = features(eg, at)
        hidden[:, at] = (gate * jax.nn.sigmoid(gate) * features(eu, at)).astype(BF16)

    every = slice(None)
    gate = features(dg, every)
    dense_hidden[...] = (gate * jax.nn.sigmoid(gate) * features(du, every)).astype(BF16)
    opening[...] = jax.nn.sigmoid(features(open_w, every))

    def branch(at):
        expert = jnp.dot(hidden[...], ed[:, at], preferred_element_type=F32)
        dense = jnp.dot(dense_hidden[...], dd[:, at], preferred_element_type=F32)
        share = share_ref[...].reshape(tokens, LANES)[:, :1]
        return expert * share + dense * opening[:, :1]

    wide = min(256, half)

    @pl.loop(0, half // wide)
    def _(j):
        src = pl.ds(pl.multiple_of(mate * half + j * wide, wide), wide)
        at = pl.ds(pl.multiple_of(j * wide, wide), wide)
        other[:, at] = branch(src).astype(BF16)

    swap = pair(other, other_in, 1)
    swap.start()

    @pl.loop(0, half // wide)
    def _(j):
        src = pl.ds(pl.multiple_of(tp * half + j * wide, wide), wide)
        at = pl.ds(pl.multiple_of(j * wide, wide), wide)
        own[:, at] = branch(src)

    swap.wait()
    summed[...] = (own[...] + other_in[...].astype(F32)).astype(BF16).reshape(n, seqs, half)
    scatter_start(n, me, tp, summed, landed, *sems(3))
    landed[me] = summed[me]
    scatter_wait(n, me, tp, summed, landed, *sems(3))
    total = lax.fori_loop(
        0, n, lambda j, acc: acc + landed[j].astype(F32), jnp.zeros((seqs, half), F32)
    )
    mine = mixed_row[:, pl.ds(pl.multiple_of(tp * half, half), half)]
    final[...] = (mine + total).astype(BF16)
    swap = pair(final, final_in, 2)
    swap.start()
    out_ref[:, pl.ds(pl.multiple_of(tp * half, half), half)] = final[...]
    swap.wait()
    out_ref[:, pl.ds(pl.multiple_of(mate * half, half), half)] = final_in[...]


def mix(n, x, retained, w_out, gain, share, open_w, weights):
    seqs, width = x.shape
    block, half, tokens = width // n, width // 2, n * seqs
    eg, eu, ed, dg, du, dd = weights
    vmem = pl.BlockSpec(memory_space=pltpu.VMEM)
    hbm = pl.BlockSpec(memory_space=pl.ANY)
    return pl.pallas_call(
        functools.partial(mix_kernel, n),
        out_shape=jax.ShapeDtypeStruct((seqs, width), BF16),
        in_specs=[vmem] * 6 + [hbm] * 6,
        out_specs=vmem,
        scratch_shapes=[
            pltpu.VMEM((n,) + retained.shape, BF16),
            pltpu.VMEM((n, seqs, block), BF16),
            pltpu.VMEM((n, seqs, block), BF16),
            pltpu.VMEM((n, seqs, block), BF16),
            pltpu.VMEM((n, seqs, block), BF16),
            pltpu.VMEM((seqs, width), F32),
            pltpu.VMEM((2, seqs, half), BF16),
            pltpu.VMEM((2, n, seqs, half), BF16),
            pltpu.VMEM(eg.shape[1:], BF16),
            pltpu.VMEM(eu.shape[1:], BF16),
            pltpu.VMEM(ed.shape[1:], BF16),
            pltpu.VMEM(dg.shape, BF16),
            pltpu.VMEM(du.shape, BF16),
            pltpu.VMEM(dd.shape, BF16),
            pltpu.VMEM((tokens, eg.shape[2]), BF16),
            pltpu.VMEM((tokens, dg.shape[1]), BF16),
            pltpu.VMEM((tokens, LANES), F32),
            pltpu.VMEM((tokens, half), BF16),
            pltpu.VMEM((tokens, half), BF16),
            pltpu.VMEM((tokens, half), F32),
            pltpu.VMEM((n, seqs, half), BF16),
            pltpu.VMEM((n, seqs, half), BF16),
            pltpu.VMEM((seqs, half), BF16),
            pltpu.VMEM((seqs, half), BF16),
            pltpu.SemaphoreType.DMA((6,)),
            pltpu.SemaphoreType.DMA((4, n)),
            pltpu.SemaphoreType.DMA((4, n)),
            pltpu.SemaphoreType.DMA((3,)),
            pltpu.SemaphoreType.DMA((3,)),
            pltpu.SemaphoreType.DMA((n,)),
            pltpu.SemaphoreType.DMA((n,)),
        ],
        compiler_params=pltpu.CompilerParams(
            collective_id=1, has_side_effects=True, vmem_limit_bytes=VMEM_LIMIT
        ),
    )(x, retained, w_out, gain, share, open_w, *weights)


def on_device(
    inputs,
    positions,
    ret_state,
    norm_mix,
    w_query,
    w_key,
    w_value,
    w_gate_in,
    head_gain,
    w_out,
    norm_ffn,
    route_ids,
    route_weight,
    exp_gate,
    exp_up,
    exp_down,
    dense_gate,
    dense_up,
    dense_down,
    branch_gate,
):
    n = lax.axis_size("ep")
    seqs, width = inputs.shape
    local_heads, head_dim = ret_state.shape[1], ret_state.shape[2]
    assert exp_gate.shape[0] == 1

    angles = rotary_angles(positions, head_dim)
    cos, sin = jnp.cos(angles), jnp.sin(angles)
    cos = jnp.concatenate([cos, cos], axis=1)
    sin = jnp.concatenate([-sin, sin], axis=1)
    gamma = jnp.exp(
        lax.dynamic_slice_in_dim(
            log_decay(HEADS), lax.axis_index("tp") * local_heads, local_heads
        )
    )
    open_w = jnp.broadcast_to(branch_gate[:, None], (width, LANES))

    joined, shares = project(
        n, inputs, norm_mix[None, :], route_ids, route_weight,
        (w_query, w_key, w_value, w_gate_in),
    )
    new_state, retained = retain(gamma, joined, head_gain[None, :], cos, sin, ret_state)
    layer_out = mix(
        n, inputs, retained, w_out, norm_ffn[None, :], shares, open_w,
        (exp_gate, exp_up, exp_down, dense_gate, dense_up, dense_down),
    )
    return (layer_out, new_state)


def solution(mesh):
    in_specs = (
        P("ep", None),
        P("ep"),
        P("ep", "tp", None, None),
        P(),
        P("ep", "tp"),
        P("ep", "tp"),
        P("ep", "tp"),
        P("ep", "tp"),
        P("tp"),
        P("tp", "ep"),
        P(),
        P("ep", None),
        P("ep", None),
        P("ep", None, "tp"),
        P("ep", None, "tp"),
        P("ep", "tp", None),
        P(None, ("ep", "tp")),
        P(None, ("ep", "tp")),
        P(("ep", "tp"), None),
        P(),
    )
    out_specs = (P("ep", None), P("ep", "tp", None, None))
    return jax.shard_map(
        on_device, mesh=mesh, in_specs=in_specs, out_specs=out_specs, check_vma=False
    )
```

profile of v0, /device:TPU:29, one launch (start us, length us, event | category | flops | bytes accessed | tf_op | source)
XLA Modules:
  0.0 110.0 jit_solution(5599057626274961713)
XLA Ops:
  0.6 0.7 convert_element_type.3
  1.3 0.1 fusion
  1.4 0.7 pad_maximum_fusion
  2.1 0.6 dynamic-slice_exponential_fusion.gamma_ref
  2.8 1.3 %broadcast_in_dim.8.gain_ref = bf16[1,2048]{1,0:T(2,128)(2,1)} reshape(bf16[2048]{0:T(1024)(128)(2,1)} %param.23) | data formatting | bytes 8192 | tf_op jit(solution)/shard_map/broadcast_in_dim | solution.py:500
  4.0 1.4 %copy.22.ids_ref = s32[16,4]{1,0:T(8,128)} copy(s32[16,4]{0,1:T(4,128)} %param.31) | data formatting | bytes 512 | tf_op args[11]
  5.4 1.3 %copy.23.weight_ref = bf16[16,4]{1,0:T(8,128)(2,1)} copy(bf16[16,4]{0,1:T(4,128)(2,1)} %param.32) | data formatting | bytes 256 | tf_op args[12]
  6.7 31.8 %shard_map.203 = (bf16[16,3072]{1,0:T(8,128)(2,1)}, f32[16,16,128]{2,1,0:T(8,128)}) custom-call(bf16[16,2048]{1,0:T(8,128)(2,1)} %x_ref.3, bf16[1,2048]{1,0:T(2,128)(2,1)} %broadcast_in_dim.8.gain_ref, s32[16,4]{1,0:T(8,128)} %copy.22.ids_ref, bf16[16,4]{1,0:T(8,128)(2,1)} %copy.23.weight_ref, bf16[128,768]{1,0:T(8,128)(2,1)} %wq.1, bf16[128,768]{1,0:T(8,128)(2,1)} %wk.1, ...), custom_call_target="tpu_custom_call" | custom-call | tf_op jit(solution)/shard_map/pallas_call | solution.py:179
  38.6 1.3 %broadcast_in_dim.18.gain_ref = bf16[1,768]{1,0:T(2,128)(2,1)} reshape(bf16[768]{0:T(1024)(128)(2,1)} %param.28) | data formatting | bytes 3072 | tf_op jit(solution)/shard_map/broadcast_in_dim | solution.py:503
  39.8 0.0 copy-start
  39.8 0.0 copy-start.1
  39.8 9.7 %shard_map.204 = (f32[16,6,128,128]{3,2,1,0:T(8,128)}, bf16[16,768]{1,0:T(8,128)(2,1)}) custom-call(f32[6]{0:T(128)} %dynamic-slice_exponential_fusion.gamma_ref, bf16[16,3072]{1,0:T(8,128)(2,1)} %get-tuple-element.6.q_ref.k_ref.v_ref.g_ref, bf16[16,3072]{1,0:T(8,128)(2,1)} %get-tuple-element.6.q_ref.k_ref.v_ref.g_ref, ...), custom_call_target="tpu_custom_call" | custom-call | tf_op jit(solution)/shard_map/pallas_call | solution.py:242
  49.5 0.0 copy-done
  49.5 1.1 %broadcast_in_dim.20.open_w = bf16[2048,128]{1,0:T(8,128)(2,1)} broadcast(bf16[2048]{0:T(1024)(128)(2,1)S(1)} %copy-done), dimensions={0} | broadcast | bytes 528384 | tf_op jit(solution)/shard_map/broadcast_in_dim | solution.py:497
  50.7 0.0 copy-done.1
  50.7 0.6 broadcast_in_dim.19.gain_ref
  51.3 57.3 %shard_map.205 = bf16[16,2048]{1,0:T(8,128)(2,1)} custom-call(bf16[16,2048]{1,0:T(8,128)(2,1)} %x_ref.3, bf16[16,768]{1,0:T(8,128)(2,1)} %get-tuple-element.7.ret_ref, bf16[768,128]{1,0:T(8,128)(2,1)} %wout_ref.1, bf16[1,2048]{1,0:T(2,128)(2,1)} %broadcast_in_dim.19.gain_ref, f32[16,16,128]{2,1,0:T(8,128)} %get-tuple-element.8.share_ref, ...), custom_call_target="tpu_custom_call" | custom-call | tf_op jit(solution)/shard_map/pallas_call | solution.py:417
  108.6 1.5 %copy.25 = bf16[16,2048]{1,0:T(8,128)(2,1)} copy(bf16[16,2048]{1,0:T(8,128)(2,1)} %shard_map.205) | data formatting | bytes 131072
  (2 shorter events, 0.0 us)
Async XLA Ops:
  39.8 9.7 %copy-start = (bf16[2048]{0:T(1024)(128)(2,1)S(1)}, bf16[2048]{0:T(1024)(128)(2,1)}, u32[]{:S(2)}) copy-start(bf16[2048]{0:T(1024)(128)(2,1)} %param.39) | copy-start | bytes 12292
  39.8 10.8 %copy-start.1 = (bf16[2048]{0:T(1024)(128)(2,1)S(1)}, bf16[2048]{0:T(1024)(128)(2,1)}, u32[]{:S(2)}) copy-start(bf16[2048]{0:T(1024)(128)(2,1)} %param.30) | copy-start | bytes 12292
where the time goes:
time: 111 us; the launch traced here: 110 us
  Pallas kernels  98.8 us (89%)
  local copies, waits for them, and re-layouts  9.11 us (8%)
  other arithmetic  1.48 us (1%)
    pallas_call x1, Pallas kernels, mix(): pl.pallas_call(functools.partial(mix_kernel, n), out_shape=jax.ShapeDtype...  57.3 us
    pallas_call x1, Pallas kernels, project(): pl.pallas_call(functools.partial(project_kernel, n), out_shape=(jax.Shape...  31.8 us
    pallas_call x1, Pallas kernels, retain(): pl.pallas_call(retain_kernel, grid=(heads,), out_shape=(jax.ShapeDtypeStr...  9.68 us
    unnamed x7, local copies, waits for them, and re-layouts  4.18 us

commit v1 on v0

v1 whole, which is shorter than its diff:
```python
import functools
import math

import jax
import jax.numpy as jnp
import numpy as np
from jax import lax
from jax.experimental import pallas as pl
from jax.experimental.pallas import tpu as pltpu
from jax.sharding import PartitionSpec as P

HEADS = 12
EPS = 1e-06
MESH = pl.DeviceIdType.MESH
LANES = 128
F32 = jnp.float32
BF16 = jnp.bfloat16
INNER = 4
CHUNKS = 2


def decay(head, head_count):
    return 1.0 - 2.0 ** (-5.0 - 5.0 * head / max(head_count - 1, 1))


def normalize(values, gain):
    return (values * lax.rsqrt(jnp.mean(values * values, axis=-1, keepdims=True) + EPS) * gain).astype(
        BF16
    )


def remote(src, dst, send, recv, ep, tp):
    return pltpu.make_async_remote_copy(
        src_ref=src,
        dst_ref=dst,
        send_sem=send,
        recv_sem=recv,
        device_id=(ep, tp),
        device_id_type=MESH,
    )


def layer_kernel(
    n, heads, dim,
    x_hbm, pos_hbm, freq_hbm, ids_hbm, weight_hbm, nmix_hbm, nffn_hbm, open_hbm, gain_hbm,
    state_hbm, wq, wk, wv, wg, wout_hbm, eg_hbm, eu_hbm, ed_hbm, dg_hbm, du_hbm, dd_hbm,
    out_ref, key_ref, value_ref,
    x_ref, pos_ref, freq_ref, ids_ref, weight_ref, nmix_ref, nffn_ref, open_ref, gain_ref,
    state, eg, eu, ed, dg, du, dd,
    xsend, xrows, wcol, wo, wo_flat, parts, zin, zsum, qkvg,
    gain_wide, table, share_out, shares, cos_ref, sin_ref, readout, kept, heads_in,
    mixs, mixin, row, half_out, gathered, open_rows, acc, hidden, dense_hidden, opening,
    other, other_in, summed, plane_in, line_out, line_in, final, final_in,
    load, xs, xr, ws, wr, local, outs, outr, shs, shr, zs, zr, ps, pr, cs, cr, ds, dr,
    ezs, eps, er, ms, mr, sws, swr, f1s, f1r, f2s, f2r, fs, fr,
):
    me, tp = lax.axis_index("ep"), lax.axis_index("tp")
    mate = 1 - tp
    outer = n // INNER
    span = outer // 2
    o, i = me // INNER, lax.rem(me, INNER)
    seqs, width = x_ref.shape
    block, half, tokens, group = width // n, width // 2, n * seqs, INNER * seqs
    kb = INNER * block
    hw = heads * dim

    small = [
        pltpu.make_async_copy(src, dst, load.at[j])
        for j, (src, dst) in enumerate(
            ((x_hbm, x_ref), (nmix_hbm, nmix_ref), (ids_hbm, ids_ref), (weight_hbm, weight_ref),
             (pos_hbm, pos_ref), (freq_hbm, freq_ref), (nffn_hbm, nffn_ref), (open_hbm, open_ref),
             (gain_hbm, gain_ref))
        )
    ]
    large = [
        pltpu.make_async_copy(src, dst, load.at[len(small) + j])
        for j, (src, dst) in enumerate(
            ((state_hbm, state), (eg_hbm.at[0], eg), (eu_hbm.at[0], eu), (dg_hbm, dg),
             (du_hbm, du), (ed_hbm.at[0], ed), (dd_hbm, dd))
        )
    ]
    for copy in small:
        copy.start()

    barrier = pltpu.get_barrier_semaphore()

    def greet(ep, core):
        pl.semaphore_signal(barrier, inc=1, device_id=(ep, core), device_id_type=MESH)

    @pl.loop(1, n)
    def _(k):
        greet(lax.rem(me + k, n), tp)

    for j in range(INNER):
        greet(o * INNER + j, mate)

    @pl.loop(1, outer)
    def _(k):
        greet(lax.rem(o + k, outer) * INNER + i, mate)

    small[0].wait()
    small[1].wait()
    normed = normalize(x_ref[...].astype(F32), nmix_ref[...].astype(F32).reshape(1, width))
    for z in range(outer):
        xsend[z] = normed[:, z * kb : (z + 1) * kb]
    pl.semaphore_wait(barrier, n - 1 + INNER + outer - 1)

    @pl.loop(1, n)
    def _(k):
        peer = lax.rem(me + k, n)
        remote(xsend.at[peer // INNER], xrows.at[me], xs.at[k], xr.at[k], peer, tp).start()

    for m, w in enumerate((wq, wk, wv, wg)):
        own_block = pltpu.make_async_copy(w, wcol.at[i], local.at[0])

        @pl.when(i != m)
        def _(m=m, w=w):
            remote(w, wcol.at[i], ws.at[m], wr.at[i], o * INNER + m, tp).start()

        @pl.when(i == m)
        def _(own_block=own_block):
            own_block.start()

    for copy in large:
        copy.start()
    xrows[me] = xsend[o]

    for j in (2, 3, 4, 5, 6, 7, 8):
        small[j].wait()
    widened = weight_ref[...].astype(F32)
    part = widened / jnp.sum(widened, axis=0, keepdims=True)
    expert = lax.broadcasted_iota(jnp.int32, (n, seqs), 0)
    named = jnp.zeros((n, seqs), F32)
    for j in range(ids_ref.shape[0]):
        named = named + jnp.where(ids_ref[j : j + 1, :] == expert, part[j : j + 1, :], 0.0)
    table[...] = jnp.zeros_like(table)
    table[:n, :seqs] = named
    share_out[...] = table[...].T[:seqs]

    @pl.loop(1, n)
    def _(k):
        peer = lax.rem(me + k, n)
        remote(share_out, shares.at[me], shs.at[k], shr.at[k], peer, tp).start()

    shares[me] = share_out[...]

    rows_at = lax.broadcasted_iota(jnp.int32, (seqs, dim), 0)
    place = jnp.zeros((seqs, dim), F32)
    for s in range(seqs):
        place = jnp.where(rows_at == s, pos_ref[s].astype(F32), place)
    angles = place * freq_ref[...]
    lower = lax.broadcasted_iota(jnp.int32, (seqs, dim), 1) < dim // 2
    cos_ref[...] = jnp.cos(angles)
    sine = jnp.sin(angles)
    sin_ref[...] = jnp.where(lower, -sine, sine)
    open_rows[...] = jnp.broadcast_to(open_ref[...].astype(F32).reshape(1, width), open_rows.shape).astype(BF16)

    gain_wide[...] = gain_ref[...].astype(F32).reshape(1, hw)

    @pl.loop(1, n)
    def _(k):
        peer, came = lax.rem(me + k, n), lax.rem(me + n - k, n)
        copy = remote(xsend.at[peer // INNER], xrows.at[came], xs.at[k], xr.at[k], peer, tp)
        copy.wait_send()
        copy.wait_recv()

    for m, w in enumerate((wq, wk, wv, wg)):
        copy = remote(w, wcol.at[m], ws.at[m], wr.at[m], o * INNER + m, tp)

        @pl.when(i != m)
        def _(copy=copy):
            copy.wait_send()
            copy.wait_recv()

        @pl.when(i == m)
        def _(m=m, w=w):
            pltpu.make_async_copy(w, wcol.at[m], local.at[0]).wait()

    product = jnp.dot(
        xrows[...].reshape(tokens, block * INNER),
        wcol[...].reshape(kb, hw),
        preferred_element_type=F32,
    )
    parts[...] = product.astype(BF16).reshape(outer, group, hw)

    def to_line(k, source):
        peer = lax.rem(o + k, outer)
        return remote(parts.at[peer], zin.at[source], zs.at[k], zr.at[k], peer * INNER + i, tp)

    @pl.loop(1, outer)
    def _(k):
        to_line(k, o).start()

    holder, slot = o // span, lax.rem(o, span)

    @pl.loop(1, outer)
    def _(k):
        peer = lax.rem(o + k, outer)
        remote(
            wout_hbm, wo.at[tp, slot], outs.at[k], outr.at[tp, slot], peer * INNER + i, holder
        ).start()

    @pl.when(holder == tp)
    def _():
        pltpu.make_async_copy(wout_hbm, wo.at[tp, slot], local.at[1]).start()

    @pl.when(holder != tp)
    def _():
        remote(wout_hbm, wo.at[tp, slot], outs.at[0], outr.at[tp, slot], me, mate).start()

    @pl.loop(1, outer)
    def _(k):
        copy = to_line(k, lax.rem(o + outer - k, outer))
        copy.wait_send()
        copy.wait_recv()

    zin[o] = parts[o]
    total = lax.fori_loop(
        0, outer, lambda z, carry: carry + zin[z].astype(F32), jnp.zeros((group, hw), F32)
    )
    zsum[...] = total.astype(BF16).reshape(INNER, seqs, hw)

    def to_plane(k, source):
        peer = lax.rem(i + k, INNER)
        return remote(zsum.at[peer], qkvg.at[source], ps.at[k], pr.at[k], o * INNER + peer, tp)

    for k in range(1, INNER):
        to_plane(k, i).start()
    qkvg[i] = zsum[i]
    large[0].wait()
    for k in range(1, INNER):
        copy = to_plane(k, lax.rem(i + INNER - k, INNER))
        copy.wait_send()
        copy.wait_recv()

    def head(h, carry):
        at = pl.ds(pl.multiple_of(h * dim, dim), dim)
        gamma = F32(0.0)
        for j in range(heads):
            low, high = decay(j, HEADS), decay(heads + j, HEADS)
            gamma = jnp.where(h == j, jnp.where(tp == 0, F32(low), F32(high)), gamma)

        def rotated(ref):
            val = ref[:, at].astype(F32)
            return val * cos_ref[...] + pltpu.roll(val, dim // 2, 1) * sin_ref[...]

        query = rotated(qkvg.at[0])
        key = rotated(qkvg.at[1]) * dim ** (-0.5)
        key_ref[:, at] = key
        value = qkvg[2, :, at].astype(F32)
        across = query.T
        for s in range(seqs):
            readout[s : s + 1, :] = jnp.sum(
                state[s, h] * across[:, s : s + 1], axis=0, keepdims=True
            )
        read = gamma * readout[...] + jnp.sum(query * key, axis=-1, keepdims=True) * value
        centred = read - jnp.mean(read, axis=-1, keepdims=True)
        scaled = centred * lax.rsqrt(jnp.mean(centred * centred, axis=-1, keepdims=True) + EPS)
        gate = qkvg[3, :, at].astype(F32)
        gain = gain_wide[:, at]
        kept[:, at] = (scaled * gain * (gate * jax.nn.sigmoid(gate))).astype(BF16)
        return carry

    lax.fori_loop(0, heads, head, 0)
    value_ref[...] = qkvg[2]

    mine = tp * INNER + i

    def to_group(src, dst, send, recv, j):
        core = lax.rem(tp + j // INNER, 2)
        peer = lax.rem(i + j % INNER, INNER)
        return remote(src(peer), dst, send.at[j], recv.at[j], o * INNER + peer, core)

    def source_of(j):
        core = lax.rem(tp + 2 - j // INNER, 2)
        return core * INNER + lax.rem(i + INNER - j % INNER, INNER)

    ring = (1, 2, 3, 4, 5, 6, 7)
    for j in ring:
        to_group(lambda p: kept, heads_in.at[mine], cs, cr, j).start()
    heads_in[mine] = kept[...]

    @pl.loop(1, outer)
    def _(k):
        peer = lax.rem(o + k, outer)
        remote(
            wout_hbm, wo.at[tp, slot], outs.at[k], outr.at[tp, slot], peer * INNER + i, holder
        ).wait_send()

    @pl.when(holder == tp)
    def _():
        pltpu.make_async_copy(wout_hbm, wo.at[tp, slot], local.at[1]).wait()

    @pl.when(holder != tp)
    def _():
        remote(wout_hbm, wo.at[tp, slot], outs.at[0], outr.at[tp, slot], me, mate).wait_send()

    for core in range(2):
        for s in range(span):

            @pl.when(jnp.logical_not(jnp.logical_and(core == tp, tp * span + s == o)))
            def _(core=core, s=s):
                remote(
                    wout_hbm, wo.at[core, s], outs.at[0], outr.at[core, s], me, mate
                ).wait_recv()

            wo_flat[core, :, s * block : (s + 1) * block] = wo[core, s]

    for j in ring:
        copy = to_group(lambda p: kept, heads_in.at[source_of(j)], cs, cr, j)
        copy.wait_send()
        copy.wait_recv()

    first, second = (
        jnp.dot(
            heads_in[c * INNER : (c + 1) * INNER].reshape(group, hw),
            wo_flat[c],
            preferred_element_type=F32,
        ).astype(BF16)
        for c in range(2)
    )
    mixs[...] = (first.astype(F32) + second.astype(F32)).astype(BF16).reshape(
        INNER, seqs, span * block
    )
    for j in ring:
        to_group(lambda p: mixs.at[p], mixin.at[mine], ds, dr, j).start()
    mixin[mine] = mixs[i]
    for j in ring:
        copy = to_group(lambda p: mixs.at[p], mixin.at[source_of(j)], ds, dr, j)
        copy.wait_send()
        copy.wait_recv()

    for z in range(outer):
        for j in range(INNER):
            b = z * INNER + j
            row[:, b * block : (b + 1) * block] = mixin[
                (z // span) * INNER + j, :, (z % span) * block : (z % span + 1) * block
            ].astype(F32)
    residual = (x_ref[...].astype(F32) + row[...]).astype(BF16).astype(F32)
    row[...] = residual
    normed = normalize(residual, nffn_ref[...].astype(F32).reshape(1, width))
    for c in range(2):
        half_out[c] = normed[:, c * half : (c + 1) * half]

    def along(k, block_id):
        peer = lax.rem(o + k, outer)
        return remote(
            half_out.at[tp], gathered.at[tp, block_id], ezs.at[k], er.at[block_id],
            peer * INNER + i, tp,
        )

    def inside(src, k, z, block_id):
        peer = lax.rem(i + k, INNER)
        return remote(
            src, gathered.at[tp, block_id], eps.at[z, k], er.at[block_id], o * INNER + peer, tp
        )

    def across_cores(half_id, block_id, k):
        return remote(
            gathered.at[tp, block_id], gathered.at[half_id, block_id], ms.at[k], mr.at[k], me, mate
        )

    @pl.loop(1, outer)
    def _(k):
        along(outer - k, me).start()

    for k in range(1, INNER):
        inside(half_out.at[tp], k, 0, me).start()
    for c in range(2):
        gathered[c, me] = half_out[c]

    def block_of(kz, ki):
        return lax.rem(o + outer - kz, outer) * INNER + lax.rem(i + INNER - ki, INNER)

    @pl.loop(1, outer)
    def _(k):
        came = block_of(k, 0)
        along(k, came).wait_recv()
        for j in range(1, INNER):
            inside(gathered.at[tp, came], j, k, came).start()
        across_cores(tp, came, k * INNER).start()

    @pl.loop(0, outer)
    def _(k):
        for j in range(1, INNER):
            came = block_of(k, j)
            inside(half_out.at[tp], j, k, came).wait_recv()
            across_cores(tp, came, k * INNER + j).start()

    for copy in large[1:]:
        copy.wait()

    cols = eg.shape[1]
    dcols = dg.shape[1]
    tile = min(256, cols)
    wide = 2 * cols

    def half_dot(c, first):
        left = gathered[c].reshape(tokens, half)
        k_at = pl.ds(pl.multiple_of(c * half, half), half)

        def put(at, value):
            if first:
                acc[:, at] = value
            else:
                acc[:, at] += value

        for base, w in ((0, eg), (cols, eu)):

            @pl.loop(0, cols // tile)
            def _(j, base=base, w=w):
                src = pl.ds(pl.multiple_of(j * tile, tile), tile)
                dst = pl.ds(pl.multiple_of(base + j * tile, tile), tile)
                put(dst, jnp.dot(left, w[k_at, src], preferred_element_type=F32))

        for base, w in ((wide, dg), (wide + dcols, du)):
            put(slice(base, base + dcols), jnp.dot(left, w[k_at, :], preferred_element_type=F32))
        put(
            slice(wide + 2 * dcols, wide + 2 * dcols + LANES),
            lax.dot_general(
                left, open_rows[:, k_at], (((1,), (1,)), ((), ())), preferred_element_type=F32
            ),
        )

    half_dot(tp, True)

    @pl.loop(1, n)
    def _(q):
        k, j = q // INNER, lax.rem(q, INNER)
        copy = across_cores(mate, block_of(k, j), q)
        copy.wait_send()
        copy.wait_recv()

    half_dot(mate, False)

    @pl.loop(1, outer)
    def _(k):
        along(k, me).wait_send()

    @pl.loop(0, outer)
    def _(k):
        for j in range(1, INNER):
            inside(half_out.at[tp], j, k, me).wait_send()

    @pl.loop(1, n)
    def _(k):
        peer, came = lax.rem(me + k, n), lax.rem(me + n - k, n)
        copy = remote(share_out, shares.at[came], shs.at[k], shr.at[k], peer, tp)
        copy.wait_send()
        copy.wait_recv()

    lane = lax.broadcasted_iota(jnp.int32, (tokens, LANES), 1)
    opening[:, :LANES] = jnp.broadcast_to(
        jnp.sum(
            jnp.where(lane == me, shares[...].reshape(tokens, LANES), 0.0), axis=-1, keepdims=True
        ),
        (tokens, LANES),
    )
    opening[:, LANES:] = jax.nn.sigmoid(acc[:, wide + 2 * dcols : wide + 2 * dcols + LANES])

    @pl.loop(0, cols // tile)
    def _(j):
        at = pl.ds(pl.multiple_of(j * tile, tile), tile)
        gate, up = acc[:, at], acc[:, pl.ds(pl.multiple_of(cols + j * tile, tile), tile)]
        hidden[:, at] = (gate * jax.nn.sigmoid(gate) * up).astype(BF16)

    gate = acc[:, wide : wide + dcols]
    dense_hidden[...] = (
        gate * jax.nn.sigmoid(gate) * acc[:, wide + dcols : wide + 2 * dcols]
    ).astype(BF16)

    piece = half // CHUNKS
    step = min(256, piece)

    def branch(at):
        expert_part = jnp.dot(hidden[...], ed[:, at], preferred_element_type=F32)
        dense_part = jnp.dot(dense_hidden[...], dd[:, at], preferred_element_type=F32)
        return expert_part * opening[:, :1] + dense_part * opening[:, LANES : LANES + 1]

    def swap(c):
        return remote(other.at[c], other_in.at[c], sws.at[c], swr.at[c], me, mate)

    for c in range(CHUNKS):

        @pl.loop(0, piece // step)
        def _(j, c=c):
            src = pl.ds(pl.multiple_of(mate * half + c * piece + j * step, step), step)
            other[c, :, pl.ds(pl.multiple_of(j * step, step), step)] = branch(src).astype(BF16)

        swap(c).start()

    def in_group(c, z, k, source):
        peer = lax.rem(i + k, INNER)
        return remote(
            summed.at[c, z, peer], plane_in.at[c, z, source], f1s.at[c, z, k], f1r.at[c, z, k],
            o * INNER + peer, tp,
        )

    def in_line(c, k, source):
        peer = lax.rem(o + k, outer)
        return remote(
            line_out.at[c, peer], line_in.at[c, source], f2s.at[c, k], f2r.at[c, k],
            peer * INNER + i, tp,
        )

    for c in range(CHUNKS):
        swap(c).wait()

        @pl.loop(0, piece // step)
        def _(j, c=c):
            src = pl.ds(pl.multiple_of(tp * half + c * piece + j * step, step), step)
            at = pl.ds(pl.multiple_of(j * step, step), step)
            both = branch(src) + other_in[c, :, at].astype(F32)
            summed[c, :, :, :, at] = both.astype(BF16).reshape(outer, INNER, seqs, step)

        @pl.loop(1, outer + 1)
        def _(k, c=c):
            z = lax.rem(o + k, outer)
            for j in range(1, INNER):
                in_group(c, z, j, i).start()

    for c in range(CHUNKS):

        @pl.loop(1, outer + 1)
        def _(k, c=c):
            z = lax.rem(o + k, outer)
            got = summed[c, z, i].astype(F32)
            for j in range(1, INNER):
                copy = in_group(c, z, j, lax.rem(i + INNER - j, INNER))
                copy.wait_send()
                copy.wait_recv()
                got = got + plane_in[c, z, lax.rem(i + INNER - j, INNER)].astype(F32)

            line_out[c, z] = got.astype(BF16)

            @pl.when(k < outer)
            def _():
                in_line(c, k, o).start()

    for c in range(CHUNKS):
        line_in[c, o] = line_out[c, o]

        @pl.loop(1, outer)
        def _(k, c=c):
            copy = in_line(c, k, lax.rem(o + outer - k, outer))
            copy.wait_send()
            copy.wait_recv()

        got = lax.fori_loop(
            0, outer, lambda z, carry, c=c: carry + line_in[c, z].astype(F32),
            jnp.zeros((seqs, piece), F32),
        )
        kept_row = row[:, pl.ds(pl.multiple_of(tp * half + c * piece, piece), piece)]
        final[:, c * piece : (c + 1) * piece] = (kept_row + got).astype(BF16)

    last = remote(final, final_in, fs, fr, me, mate)
    last.start()
    out_ref[:, pl.ds(pl.multiple_of(tp * half, half), half)] = final[...]
    last.wait()
    out_ref[:, pl.ds(pl.multiple_of(mate * half, half), half)] = final_in[...]


def layer(n, args):
    x, pos, freq, ids, weight, nmix, nffn, opened, gain, state = args[:10]
    wq, wout, eg, ed, dg, dd = args[10], args[14], args[15], args[17], args[18], args[20]
    seqs, width = x.shape
    heads, dim = state.shape[1], state.shape[2]
    hw, block, half, tokens = heads * dim, width // n, width // 2, n * seqs
    outer = n // INNER
    span, group, kb, piece = outer // 2, INNER * seqs, INNER * block, half // CHUNKS
    cols, dcols = eg.shape[2], dg.shape[1]
    vm, sem = pltpu.VMEM, pltpu.SemaphoreType.DMA
    vmem = pl.BlockSpec(memory_space=pltpu.VMEM)
    hbm = pl.BlockSpec(memory_space=pl.ANY)
    return pl.pallas_call(
        functools.partial(layer_kernel, n, heads, dim),
        out_shape=(
            jax.ShapeDtypeStruct((seqs, width), BF16),
            jax.ShapeDtypeStruct((seqs, hw), F32),
            jax.ShapeDtypeStruct((seqs, hw), BF16),
        ),
        in_specs=[hbm] * len(args),
        out_specs=(vmem, vmem, vmem),
        scratch_shapes=[
            vm(x.shape, BF16), pltpu.SMEM(pos.shape, jnp.int32), vm(freq.shape, F32),
            vm(ids.shape, jnp.int32), vm(weight.shape, BF16), vm(nmix.shape, BF16),
            vm(nffn.shape, BF16), vm(opened.shape, BF16), vm(gain.shape, BF16),
            vm(state.shape, F32), vm(eg.shape[1:], BF16), vm(eg.shape[1:], BF16),
            vm(ed.shape[1:], BF16), vm(dg.shape, BF16), vm(dg.shape, BF16), vm(dd.shape, BF16),
            vm((outer, seqs, kb), BF16),
            vm((n, seqs, kb), BF16),
            vm((INNER, block, hw), BF16),
            vm((2, span, hw, block), BF16),
            vm((2, hw, span * block), BF16),
            vm((outer, group, hw), BF16),
            vm((outer, group, hw), BF16),
            vm((INNER, seqs, hw), BF16),
            vm((INNER, seqs, hw), BF16),
            vm((1, hw), F32),
            vm((LANES, LANES), F32),
            vm((seqs, LANES), F32),
            vm((n, seqs, LANES), F32),
            vm((seqs, dim), F32), vm((seqs, dim), F32), vm((seqs, dim), F32),
            vm((seqs, hw), BF16),
            vm((2 * INNER, seqs, hw), BF16),
            vm((INNER, seqs, span * block), BF16),
            vm((2 * INNER, seqs, span * block), BF16),
            vm((seqs, width), F32),
            vm((2, seqs, half), BF16),
            vm((2, n, seqs, half), BF16),
            vm((LANES, width), BF16),
            vm((tokens, 2 * cols + 2 * dcols + LANES), F32),
            vm((tokens, cols), BF16),
            vm((tokens, dcols), BF16),
            vm((tokens, 2 * LANES), F32),
            vm((CHUNKS, tokens, piece), BF16),
            vm((CHUNKS, tokens, piece), BF16),
            vm((CHUNKS, outer, INNER, seqs, piece), BF16),
            vm((CHUNKS, outer, INNER, seqs, piece), BF16),
            vm((CHUNKS, outer, seqs, piece), BF16),
            vm((CHUNKS, outer, seqs, piece), BF16),
            vm((seqs, half), BF16),
            vm((seqs, half), BF16),
            sem((16,)),
            sem((n,)), sem((n,)),
            sem((INNER,)), sem((INNER,)), sem((2,)),
            sem((outer,)), sem((2, span)),
            sem((n,)), sem((n,)),
            sem((outer,)), sem((outer,)),
            sem((INNER,)), sem((INNER,)),
            sem((2 * INNER,)), sem((2 * INNER,)),
            sem((2 * INNER,)), sem((2 * INNER,)),
            sem((outer,)), sem((outer, INNER)), sem((n,)),
            sem((n,)), sem((n,)),
            sem((CHUNKS,)), sem((CHUNKS,)),
            sem((CHUNKS, outer, INNER)), sem((CHUNKS, outer, INNER)),
            sem((CHUNKS, outer)), sem((CHUNKS, outer)),
            sem, sem,
        ],
        compiler_params=pltpu.CompilerParams(
            collective_id=0, has_side_effects=True, vmem_limit_bytes=(40 if n <= 16 else 60) * 2**20
        ),
        name="layer",
    )(*args)


def update_kernel(heads, out_in, key_ref, value_ref, state_ref, out_ref, new_ref):
    h = pl.program_id(0)
    seqs = key_ref.shape[0]
    tp = lax.axis_index("tp")
    gamma = F32(0.0)
    for j in range(heads):
        low, high = decay(j, HEADS), decay(heads + j, HEADS)
        gamma = jnp.where(h == j, jnp.where(tp == 0, F32(low), F32(high)), gamma)

    @pl.when(h == 0)
    def _():
        out_ref[...] = out_in[...]

    key = key_ref[...].T
    value = value_ref[...].astype(F32)
    for s in range(seqs):
        new_ref[s, 0] = gamma * state_ref[s, 0] + key[:, s : s + 1] * value[s : s + 1, :]


def update(out, key, value, state):
    seqs, heads, dim = state.shape[:3]
    held = pl.BlockSpec((seqs, 1, dim, dim), lambda h: (0, h, 0, 0))
    piece = pl.BlockSpec((seqs, dim), lambda h: (0, h))
    whole = pl.BlockSpec(out.shape, lambda h: (0, 0))
    return pl.pallas_call(
        functools.partial(update_kernel, heads),
        grid=(heads,),
        out_shape=(
            jax.ShapeDtypeStruct(out.shape, BF16),
            jax.ShapeDtypeStruct(state.shape, F32),
        ),
        in_specs=[whole, piece, piece, held],
        out_specs=(whole, held),
        compiler_params=pltpu.CompilerParams(vmem_limit_bytes=16 * 2**20),
        name="update",
    )(out, key, value, state)


def on_device(
    inputs,
    positions,
    ret_state,
    norm_mix,
    w_query,
    w_key,
    w_value,
    w_gate_in,
    head_gain,
    w_out,
    norm_ffn,
    route_ids,
    route_weight,
    exp_gate,
    exp_up,
    exp_down,
    dense_gate,
    dense_up,
    dense_down,
    branch_gate,
):
    n = lax.axis_size("ep")
    dim = ret_state.shape[2]
    assert exp_gate.shape[0] == 1 and n % (2 * INNER) == 0 and n <= LANES
    turns = 10000.0 ** (-2.0 * np.arange(dim // 2) / dim)
    freq = jnp.asarray(np.concatenate([turns, turns])[None].astype(np.float32))
    out, key, value = layer(
        n,
        (inputs, positions, freq, route_ids.T, route_weight.T, norm_mix, norm_ffn, branch_gate,
         head_gain, ret_state, w_query, w_key, w_value, w_gate_in, w_out, exp_gate, exp_up,
         exp_down, dense_gate, dense_up, dense_down),
    )
    return update(out, key, value, ret_state)


def solution(mesh):
    in_specs = (
        P("ep", None),
        P("ep"),
        P("ep", "tp", None, None),
        P(),
        P("ep", "tp"),
        P("ep", "tp"),
        P("ep", "tp"),
        P("ep", "tp"),
        P("tp"),
        P("tp", "ep"),
        P(),
        P("ep", None),
        P("ep", None),
        P("ep", None, "tp"),
        P("ep", None, "tp"),
        P("ep", "tp", None),
        P(None, ("ep", "tp")),
        P(None, ("ep", "tp")),
        P(("ep", "tp"), None),
        P(),
    )
    out_specs = (P("ep", None), P("ep", "tp", None, None))
    return jax.shard_map(
        on_device, mesh=mesh, in_specs=in_specs, out_specs=out_specs, check_vma=False
    )
```

time: 111 us -> 110 us (level)
  the two profiles are of different devices: /device:TPU:29 before, /device:TPU:0 now
where the time goes in v1:
time: 110 us; the launch traced here: 109 us
  Pallas kernels  89.4 us (81%)
  local copies, waits for them, and re-layouts  19.1 us (17%)
    pallas_call x1, Pallas kernels, layer(): pl.pallas_call(functools.partial(layer_kernel, n, heads, dim), out_shape=...  84.2 us
    unnamed x44, local copies, waits for them, and re-layouts  19.1 us
    pallas_call x1, Pallas kernels, update(): pl.pallas_call(functools.partial(update_kernel, heads), grid=(heads,), ou...  5.18 us

profile of v1, /device:TPU:0, one launch (start us, length us, event | category | flops | bytes accessed | tf_op | source)
XLA Modules:
  0.0 109.1 jit_solution(12557056603900342364)
XLA Ops:
  0.6 0.0 slice-start
  0.6 0.0 copy-start
  0.7 1.7 %copy-done = bf16[1,2048,512]{2,1,0:T(8,128)(2,1)S(1)} copy-done((bf16[1,2048,512]{2,1,0:T(8,128)(2,1)S(1)}, bf16[1,2048,512]{2,1,0:T(8,128)(2,1)}, u32[]{:S(2)}) %copy-start) | copy-done | bytes 2097176
  2.4 1.7 %copy-done.1 = bf16[1,2048,512]{2,1,0:T(8,128)(2,1)S(1)} copy-done((bf16[1,2048,512]{2,1,0:T(8,128)(2,1)S(1)}, bf16[1,2048,512]{2,1,0:T(8,128)(2,1)}, u32[]{:S(2)}) %copy-start.1) | copy-done | bytes 2097176
  4.1 1.6 %copy-done.2 = bf16[1,512,2048]{2,1,0:T(8,128)(2,1)S(1)} copy-done((bf16[1,512,2048]{2,1,0:T(8,128)(2,1)S(1)}, bf16[1,512,2048]{2,1,0:T(8,128)(2,1)}, u32[]{:S(2)}) %copy-start.2) | copy-done | bytes 2097176
  5.7 1.0 copy-done.3
  6.8 1.0 copy-done.4
  7.8 1.0 copy-done.5
  8.8 0.9 copy-done.6
  9.8 0.9 copy-done.7
  10.7 0.9 copy-done.8
  11.6 0.9 copy-done.9
  12.6 0.9 copy-done.10
  13.5 0.8 copy-done.11
  14.3 0.7 copy-done.12
  15.0 0.7 copy-done.13
  15.7 0.7 copy-done.14
  16.4 0.7 copy-done.15
  17.1 0.7 copy-done.16
  17.7 0.7 copy-done.17
  18.4 0.7 copy-done.18
  19.1 0.7 copy-done.19
  19.7 84.2 %layer.1 = (bf16[16,2048]{1,0:T(8,128)(2,1)S(1)}, f32[16,768]{1,0:T(8,128)S(1)}, bf16[16,768]{1,0:T(8,128)(2,1)S(1)}) custom-call(bf16[16,2048]{1,0:T(8,128)(2,1)S(1)} %copy-done.11, s32[16]{0:T(128)S(1)} %copy-done.18, f32[1,128]{1,0:T(1,128)S(1)} %copy-done.19, s32[4,16]{1,0:T(4,128)S(1)} %bitcast.4, bf16[4,16]{1,0:T(4,128)(2,1)S(1)} %bitcast.5, ...), custom_call_target="tpu_custom_call" | custom-call | tf_op jit(solution)/shard_map/layer/pallas_call | solution.py:575
  104.0 5.2 %update.1 = (bf16[16,2048]{1,0:T(8,128)(2,1)}, f32[16,6,128,128]{3,2,1,0:T(8,128)}) custom-call(bf16[16,2048]{1,0:T(8,128)(2,1)S(1)} %get-tuple-element.5.out_in, f32[16,768]{1,0:T(8,128)S(1)} %get-tuple-element.6.key_ref, bf16[16,768]{1,0:T(8,128)(2,1)S(1)} %get-tuple-element.7.value_ref, f32[16,6,128,128]{3,2,1,0:T(8,128)S(1)} %bitcast.3), custom_call_target="tpu_custom_call" | custom-call | tf_op jit(solution)/shard_map/update/pallas_call | solution.py:671
  (23 shorter events, 0.0 us)
Async XLA Ops:
  0.6 103.3 %slice-start = ((s8[6291456]{0:T(1024)(128)(4,1)}), s8[4194304]{0:T(1024)(128)(4,1)S(1)}, s32[]{:S(2)}) async-start(s8[6291456]{0:T(1024)(128)(4,1)} %bitcast.2), calls=%async_computation | async-start | bytes 8388608
  0.6 1.7 %copy-start = (bf16[1,2048,512]{2,1,0:T(8,128)(2,1)S(1)}, bf16[1,2048,512]{2,1,0:T(8,128)(2,1)}, u32[]{:S(2)}) copy-start(bf16[1,2048,512]{2,1,0:T(8,128)(2,1)} %eg_hbm.1) | copy-start | bytes 6291460
  2.4 1.7 %copy-start.1 = (bf16[1,2048,512]{2,1,0:T(8,128)(2,1)S(1)}, bf16[1,2048,512]{2,1,0:T(8,128)(2,1)}, u32[]{:S(2)}) copy-start(bf16[1,2048,512]{2,1,0:T(8,128)(2,1)} %eu_hbm.1) | copy-start | bytes 6291460
  4.1 1.6 %copy-start.2 = (bf16[1,512,2048]{2,1,0:T(8,128)(2,1)S(1)}, bf16[1,512,2048]{2,1,0:T(8,128)(2,1)}, u32[]{:S(2)}) copy-start(bf16[1,512,2048]{2,1,0:T(8,128)(2,1)} %ed_hbm.1) | copy-start | bytes 6291460
  5.7 1.0 copy-start.3
  6.8 1.0 copy-start.4
  7.8 1.0 copy-start.5
  8.8 0.9 copy-start.6
  9.8 0.9 copy-start.7
  10.7 0.9 copy-start.8
  11.6 0.9 copy-start.9
  12.6 0.9 copy-start.10
  13.5 0.8 copy-start.11
  14.3 0.7 copy-start.12
  15.0 0.7 copy-start.13
  15.7 0.7 copy-start.14
  16.4 0.7 copy-start.15
  17.1 0.7 copy-start.16
  17.7 0.7 copy-start.17
  18.4 0.7 copy-start.18
  19.1 0.7 copy-start.19
  19.7 84.2 %slice-start.1 = ((s8[6291456]{0:T(1024)(128)(4,1)}), s8[2097152]{0:T(1024)(128)(4,1)S(1)}, s32[]{:S(2)}) async-start(s8[6291456]{0:T(1024)(128)(4,1)} %bitcast.2), calls=%async_computation.1 | async-start | bytes 4194304

commit v2 on v1

v2 whole, which is shorter than its diff:
```python
import functools
import math

import jax
import jax.numpy as jnp
import numpy as np
from jax import lax
from jax.experimental import pallas as pl
from jax.experimental.pallas import tpu as pltpu
from jax.sharding import PartitionSpec as P

HEADS = 12
EPS = 1e-06
MESH = pl.DeviceIdType.MESH
LANES = 128
F32 = jnp.float32
BF16 = jnp.bfloat16
INNER = 4
CHUNKS = 2
WIDE = 256
PIECES = 3


def decay(head, head_count):
    return 1.0 - 2.0 ** (-5.0 - 5.0 * head / max(head_count - 1, 1))


def normalize(values, gain):
    return (values * lax.rsqrt(jnp.mean(values * values, axis=-1, keepdims=True) + EPS) * gain).astype(
        BF16
    )


def split(values):
    rest, pieces = values, []
    for _ in range(PIECES):
        pieces.append(rest.astype(BF16).astype(F32))
        rest = rest - pieces[-1]
    return jnp.concatenate(pieces, axis=0)


def remote(src, dst, send, recv, ep, tp):
    return pltpu.make_async_remote_copy(
        src_ref=src,
        dst_ref=dst,
        send_sem=send,
        recv_sem=recv,
        device_id=(ep, tp),
        device_id_type=MESH,
    )


def layer_kernel(
    n, heads, dim,
    x_hbm, pos_hbm, freq_hbm, ids_hbm, weight_hbm, nmix_hbm, nffn_hbm, open_hbm, gain_hbm,
    state_hbm, wq, wk, wv, wg, wout_hbm, eg_hbm, eu_hbm, ed_hbm, dg_hbm, du_hbm, dd_hbm,
    out_ref, key_ref, value_ref,
    x_ref, pos_ref, freq_ref, ids_ref, weight_ref, nmix_ref, nffn_ref, open_ref, gain_ref,
    state, eg, eu, ed, dg, du, dd,
    xsend, xrows, spread, wcol, wo, wo_flat, parts, zin, zsum, qkvg,
    gain_wide, table, share_rows, shares, cos_ref, sin_ref, readout, kept, heads_in,
    mixs, mixin, row, half_out, gathered, open_rows, acc, hidden, dense_hidden, opening,
    other, other_in, summed, plane_in, line_out, line_in, final, final_in,
    load, xs, xr, xm, ws, wr, local, outs, outr, shs, shr, zs, zr, ps, pr, cs, cr, ds, dr,
    ezs, eps, er, ms, mr, sws, swr, f1s, f1r, f2s, f2r, fs, fr,
):
    me, tp = lax.axis_index("ep"), lax.axis_index("tp")
    mate = 1 - tp
    outer = n // INNER
    span = INNER // 2
    o, i = me // INNER, lax.rem(me, INNER)
    seqs, width = x_ref.shape
    block, half, tokens, group = width // n, width // 2, n * seqs, INNER * seqs
    kb = INNER * block
    hw = heads * dim
    slabs, per_slab = hw // WIDE, WIDE // dim

    small = [
        pltpu.make_async_copy(src, dst, load.at[j])
        for j, (src, dst) in enumerate(
            ((x_hbm, x_ref), (nmix_hbm, nmix_ref), (ids_hbm, ids_ref), (weight_hbm, weight_ref),
             (pos_hbm, pos_ref), (freq_hbm, freq_ref), (nffn_hbm, nffn_ref), (open_hbm, open_ref),
             (gain_hbm, gain_ref))
        )
    ]
    large = [
        pltpu.make_async_copy(src, dst, load.at[len(small) + j])
        for j, (src, dst) in enumerate(
            ((state_hbm, state), (eg_hbm.at[0], eg), (eu_hbm.at[0], eu), (dg_hbm, dg),
             (du_hbm, du), (ed_hbm.at[0], ed), (dd_hbm, dd))
        )
    ]
    for copy in small:
        copy.start()

    barrier = pltpu.get_barrier_semaphore()

    def greet(ep, core):
        pl.semaphore_signal(barrier, inc=1, device_id=(ep, core), device_id_type=MESH)

    @pl.loop(1, n)
    def _(k):
        greet(lax.rem(me + k, n), tp)

    for j in range(INNER):
        greet(o * INNER + j, mate)

    @pl.loop(1, outer)
    def _(k):
        greet(lax.rem(o + k, outer) * INNER + i, mate)

    small[0].wait()
    small[1].wait()
    normed = normalize(x_ref[...].astype(F32), nmix_ref[...].astype(F32).reshape(1, width))
    for z in range(outer):
        for c in range(2):
            xsend[z, c] = normed[:, z * kb + c * (kb // 2) : z * kb + (c + 1) * (kb // 2)]
    pl.semaphore_wait(barrier, n - 1 + INNER + outer - 1)

    @pl.loop(1, n)
    def _(k):
        peer = lax.rem(me + k, n)
        remote(
            xsend.at[peer // INNER, tp], xrows.at[tp, me], xs.at[k], xr.at[k], peer, tp
        ).start()

    def rows_of(c, m, w, source):
        return remote(
            w.at[:, c * WIDE : (c + 1) * WIDE], wcol.at[c, source], ws.at[c, m], wr.at[c, source],
            o * INNER + m, tp,
        )

    def own_rows(c, m, w):
        return pltpu.make_async_copy(w.at[:, c * WIDE : (c + 1) * WIDE], wcol.at[c, m], local.at[c])

    for c in range(slabs):
        for m, w in enumerate((wq, wk, wv, wg)):

            @pl.when(i != m)
            def _(c=c, m=m, w=w):
                rows_of(c, m, w, i).start()

            @pl.when(i == m)
            def _(c=c, m=m, w=w):
                own_rows(c, m, w).start()

    holder, slot = i // span, lax.rem(i, span)

    def block_to(k):
        peer = lax.rem(i + k, INNER)
        return remote(
            wout_hbm, wo.at[tp, slot], outs.at[k], outr.at[tp, slot], o * INNER + peer, holder
        )

    own_wout = pltpu.make_async_copy(wout_hbm, wo.at[tp, slot], local.at[slabs])
    mate_wout = remote(wout_hbm, wo.at[tp, slot], outs.at[0], outr.at[tp, slot], me, mate)

    for k in range(1, INNER):
        block_to(k).start()

    @pl.when(holder == tp)
    def _():
        own_wout.start()

    @pl.when(holder != tp)
    def _():
        mate_wout.start()

    for copy in large:
        copy.start()
    xrows[tp, me] = xsend[o, tp]

    for j in (2, 3, 4, 5, 6, 7, 8):
        small[j].wait()
    widened = weight_ref[...].astype(F32)
    part = widened / jnp.sum(widened, axis=0, keepdims=True)
    expert = lax.broadcasted_iota(jnp.int32, (n, seqs), 0)
    named = jnp.zeros((n, seqs), F32)
    for j in range(ids_ref.shape[0]):
        named = named + jnp.where(ids_ref[j : j + 1, :] == expert, part[j : j + 1, :], 0.0)
    table[...] = jnp.zeros_like(table)
    table[:n, :seqs] = named
    for j in range(n):
        share_rows[j] = table[j : j + 1, :]

    def share_to(k, source):
        peer = lax.rem(me + k, n)
        return remote(share_rows.at[peer], shares.at[source], shs.at[k], shr.at[k], peer, tp)

    @pl.loop(1, n)
    def _(k):
        share_to(k, me).start()

    shares[me] = share_rows[me]

    rows_at = lax.broadcasted_iota(jnp.int32, (seqs, dim), 0)
    place = jnp.zeros((seqs, dim), F32)
    for s in range(seqs):
        place = jnp.where(rows_at == s, pos_ref[s].astype(F32), place)
    angles = place * freq_ref[...]
    lower = lax.broadcasted_iota(jnp.int32, (seqs, dim), 1) < dim // 2
    cos_ref[...] = jnp.cos(angles)
    sine = jnp.sin(angles)
    sin_ref[...] = jnp.where(lower, -sine, sine)
    open_rows[...] = jnp.broadcast_to(open_ref[...].astype(F32).reshape(1, width), open_rows.shape).astype(BF16)

    apart = lax.rem(lax.broadcasted_iota(jnp.int32, spread.shape, 0), seqs)
    spread[...] = jnp.where(
        apart == lax.broadcasted_iota(jnp.int32, spread.shape, 1) // dim, 1.0, 0.0
    ).astype(BF16)
    gain_wide[...] = gain_ref[...].astype(F32).reshape(1, hw)

    @pl.loop(1, n)
    def _(k):
        peer, came = lax.rem(me + k, n), lax.rem(me + n - k, n)
        copy = remote(
            xsend.at[peer // INNER, tp], xrows.at[tp, came], xs.at[k], xr.at[k], peer, tp
        )
        copy.wait_send()
        copy.wait_recv()

    def rows_to_mate(c):
        return remote(xrows.at[tp], xrows.at[c], xm.at[0], xm.at[1], me, mate)

    rows_to_mate(tp).start()

    def to_line(c, k, source):
        peer = lax.rem(o + k, outer)
        return remote(
            parts.at[c, peer], zin.at[c, source], zs.at[c, k], zr.at[c, k], peer * INNER + i, tp
        )

    for c in range(slabs):
        for m, w in enumerate((wq, wk, wv, wg)):

            @pl.when(i != m)
            def _(c=c, m=m, w=w):
                copy = rows_of(c, m, w, m)
                copy.wait_send()
                copy.wait_recv()

            @pl.when(i == m)
            def _(c=c, m=m, w=w):
                own_rows(c, m, w).wait()

        if c == 0:
            swapped = rows_to_mate(mate)
            swapped.wait_send()
            swapped.wait_recv()
        product = sum(
            jnp.dot(
                xrows[q].reshape(tokens, kb // 2),
                wcol[c, q * 2 : q * 2 + 2].reshape(kb // 2, WIDE),
                preferred_element_type=F32,
            )
            for q in range(2)
        )
        parts[c] = product.astype(BF16).reshape(outer, group, WIDE)

        @pl.loop(1, outer)
        def _(k, c=c):
            to_line(c, k, o).start()

    def to_plane(c, k, source):
        peer = lax.rem(i + k, INNER)
        return remote(
            zsum.at[c, peer], qkvg.at[c, source], ps.at[c, k], pr.at[c, k], o * INNER + peer, tp
        )

    def head(c, q):
        h = c * per_slab + q
        at = slice(q * dim, (q + 1) * dim)
        gamma = jnp.where(tp == 0, F32(decay(h, HEADS)), F32(decay(heads + h, HEADS)))

        def rotated(j):
            val = qkvg[c, j, :, at].astype(F32)
            return val * cos_ref[...] + pltpu.roll(val, dim // 2, 1) * sin_ref[...]

        query = rotated(0)
        key = rotated(1) * dim ** (-0.5)
        key_ref[:, h * dim : (h + 1) * dim] = key
        value = qkvg[c, 2, :, at].astype(F32)
        value_ref[:, h * dim : (h + 1) * dim] = qkvg[c, 2, :, at]
        across = split(query).T.astype(BF16)
        for s in range(0, seqs, 2):
            wide = jnp.dot(
                across, spread[:, s * dim : (s + 2) * dim], preferred_element_type=F32
            )
            for t in range(2):
                readout[s + t : s + t + 1, :] = jnp.sum(
                    state[s + t, h] * wide[:, t * dim : (t + 1) * dim], axis=0, keepdims=True
                )
        read = gamma * readout[...] + jnp.sum(query * key, axis=-1, keepdims=True) * value
        centred = read - jnp.mean(read, axis=-1, keepdims=True)
        scaled = centred * lax.rsqrt(jnp.mean(centred * centred, axis=-1, keepdims=True) + EPS)
        gate = qkvg[c, 3, :, at].astype(F32)
        gain = gain_wide[:, h * dim : (h + 1) * dim]
        kept[c, :, at] = (scaled * gain * (gate * jax.nn.sigmoid(gate))).astype(BF16)

    mine = tp * outer + o

    def to_cores(src, dst, send, recv, j):
        core = lax.rem(tp + j // outer, 2)
        peer = lax.rem(o + lax.rem(j, outer), outer)
        return remote(src(peer), dst, send.at[j], recv.at[j], peer * INNER + i, core)

    def source_of(j):
        core = lax.rem(tp + 2 - j // outer, 2)
        return core * outer + lax.rem(o + outer - lax.rem(j, outer), outer)

    def kept_to(c, j, source):
        return to_cores(lambda p: kept.at[c], heads_in.at[c, source], cs.at[c], cr.at[c], j)

    def retain(c):
        for k in range(1, INNER):
            copy = to_plane(c, k, lax.rem(i + INNER - k, INNER))
            copy.wait_send()
            copy.wait_recv()
        for q in range(per_slab):
            head(c, q)

        @pl.loop(1, 2 * outer)
        def _(j):
            kept_to(c, j, mine).start()

        heads_in[c, mine] = kept[c]

    large[0].wait()
    for c in range(slabs):

        @pl.loop(1, outer)
        def _(k, c=c):
            copy = to_line(c, k, lax.rem(o + outer - k, outer))
            copy.wait_send()
            copy.wait_recv()

        zin[c, o] = parts[c, o]
        total = lax.fori_loop(
            0, outer, lambda z, carry, c=c: carry + zin[c, z].astype(F32),
            jnp.zeros((group, WIDE), F32),
        )
        zsum[c] = total.astype(BF16).reshape(INNER, seqs, WIDE)
        for k in range(1, INNER):
            to_plane(c, k, i).start()
        qkvg[c, i] = zsum[c, i]
        if c > 0:
            retain(c - 1)
    retain(slabs - 1)

    for k in range(1, INNER):
        block_to(k).wait_send()

    @pl.when(holder == tp)
    def _():
        own_wout.wait()

    @pl.when(holder != tp)
    def _():
        mate_wout.wait_send()

    for core in range(2):
        for s in range(span):

            @pl.when(jnp.logical_not(jnp.logical_and(core == tp, tp * span + s == i)))
            def _(core=core, s=s):
                remote(
                    wout_hbm, wo.at[core, s], outs.at[0], outr.at[core, s], me, mate
                ).wait_recv()

            wo_flat[core, :, s * block : (s + 1) * block] = wo[core, s]

    for c in range(slabs):

        @pl.loop(1, 2 * outer)
        def _(j, c=c):
            copy = kept_to(c, j, source_of(j))
            copy.wait_send()
            copy.wait_recv()

    first, second = (
        sum(
            jnp.dot(
                heads_in[c, q * outer : (q + 1) * outer].reshape(outer * seqs, WIDE),
                wo_flat[q, c * WIDE : (c + 1) * WIDE, :],
                preferred_element_type=F32,
            )
            for c in range(slabs)
        ).astype(BF16)
        for q in range(2)
    )
    mixs[...] = (first.astype(F32) + second.astype(F32)).astype(BF16).reshape(
        outer, seqs, span * block
    )

    def mixed_to(j, source):
        return to_cores(lambda p: mixs.at[p], mixin.at[source], ds, dr, j)

    @pl.loop(1, 2 * outer)
    def _(j):
        mixed_to(j, mine).start()

    mixin[mine] = mixs[o]
    @pl.loop(1, 2 * outer)
    def _(j):
        copy = mixed_to(j, source_of(j))
        copy.wait_send()
        copy.wait_recv()

    for z in range(outer):
        for j in range(INNER):
            b = z * INNER + j
            row[:, b * block : (b + 1) * block] = mixin[
                (j // span) * outer + z, :, (j % span) * block : (j % span + 1) * block
            ].astype(F32)
    residual = (x_ref[...].astype(F32) + row[...]).astype(BF16).astype(F32)
    row[...] = residual
    normed = normalize(residual, nffn_ref[...].astype(F32).reshape(1, width))
    for c in range(2):
        half_out[c] = normed[:, c * half : (c + 1) * half]

    def along(peer, block_id):
        return remote(
            half_out.at[tp], gathered.at[tp, block_id], ezs.at[peer], er.at[block_id],
            peer * INNER + i, tp,
        )

    def inside(src, k, z, block_id):
        peer = lax.rem(i + k, INNER)
        return remote(
            src, gathered.at[tp, block_id], eps.at[z, k], er.at[block_id], o * INNER + peer, tp
        )

    def across_cores(half_id, block_id):
        return remote(
            gathered.at[tp, block_id], gathered.at[half_id, block_id], ms.at[block_id],
            mr.at[block_id], me, mate,
        )

    def on_line(far, act):
        for sign in (1, -1):
            peer = o + sign * far

            @pl.when(jnp.logical_and(peer >= 0, peer < outer))
            def _(peer=peer):
                act(peer)

    @pl.loop(1, outer)
    def _(d):
        on_line(outer - d, lambda peer: along(peer, me).start())

    for k in range(1, INNER):
        inside(half_out.at[tp], k, o, me).start()
    for c in range(2):
        gathered[c, me] = half_out[c]

    def from_group(z):
        for j in range(1, INNER):
            came = z * INNER + lax.rem(i + INNER - j, INNER)
            inside(half_out.at[tp], j, z, came).wait_recv()
            across_cores(tp, came).start()

    def relay(peer):
        came = peer * INNER + i
        along(peer, came).wait_recv()
        for j in range(1, INNER):
            inside(gathered.at[tp, came], j, peer, came).start()
        across_cores(tp, came).start()

    cols = eg.shape[1]
    dcols = dg.shape[1]
    tile = min(256, cols)
    wide = 2 * cols
    part_rows = tokens // 2
    near = o // (outer // 2)

    def half_dot(g, c, first):
        per = n // 2
        left = gathered[c, pl.ds(g * per, per)].reshape(part_rows, half)
        k_at = pl.ds(pl.multiple_of(c * half, half), half)
        rows = pl.ds(pl.multiple_of(g * part_rows, part_rows), part_rows)

        def put(at, value):
            if first:
                acc[rows, at] = value
            else:
                acc[rows, at] += value

        for base, w in ((0, eg), (cols, eu)):

            @pl.loop(0, cols // tile)
            def _(j, base=base, w=w):
                src = pl.ds(pl.multiple_of(j * tile, tile), tile)
                dst = pl.ds(pl.multiple_of(base + j * tile, tile), tile)
                put(dst, jnp.dot(left, w[k_at, src], preferred_element_type=F32))

        for base, w in ((wide, dg), (wide + dcols, du)):
            put(slice(base, base + dcols), jnp.dot(left, w[k_at, :], preferred_element_type=F32))
        put(
            slice(wide + 2 * dcols, wide + 2 * dcols + LANES),
            lax.dot_general(
                left, open_rows[:, k_at], (((1,), (1,)), ((), ())), preferred_element_type=F32
            ),
        )

    def from_mate(g):
        @pl.loop(0, n // 2)
        def _(q):
            block_id = g * (n // 2) + q

            @pl.when(block_id != me)
            def _():
                copy = across_cores(mate, block_id)
                copy.wait_send()
                copy.wait_recv()

    @pl.loop(1, outer)
    def _(d):
        on_line(d, relay)

    @pl.loop(0, outer // 2)
    def _(z):
        from_group(near * (outer // 2) + z)

    for copy in large[1:]:
        copy.wait()

    half_dot(near, tp, True)
    from_mate(near)
    half_dot(near, mate, False)
    away = 1 - near

    @pl.loop(0, outer // 2)
    def _(z):
        from_group(away * (outer // 2) + z)

    half_dot(away, tp, True)
    from_mate(away)
    half_dot(away, mate, False)

    @pl.loop(1, outer)
    def _(d):
        on_line(d, lambda peer: along(peer, me).wait_send())

    @pl.loop(0, outer)
    def _(z):
        for j in range(1, INNER):
            inside(half_out.at[tp], j, z, me).wait_send()

    @pl.loop(1, n)
    def _(k):
        copy = share_to(k, lax.rem(me + n - k, n))
        copy.wait_send()
        copy.wait_recv()

    for j in range(n):
        table[j : j + 1, :] = shares[j]
    columns = table[...].T[:seqs]
    for j in range(n):
        opening[j * seqs : (j + 1) * seqs, :LANES] = jnp.broadcast_to(
            columns[:, j : j + 1], (seqs, LANES)
        )
    opening[:, LANES:] = jax.nn.sigmoid(acc[:, wide + 2 * dcols : wide + 2 * dcols + LANES])

    @pl.loop(0, cols // tile)
    def _(j):
        at = pl.ds(pl.multiple_of(j * tile, tile), tile)
        gate, up = acc[:, at], acc[:, pl.ds(pl.multiple_of(cols + j * tile, tile), tile)]
        hidden[:, at] = (gate * jax.nn.sigmoid(gate) * up).astype(BF16)

    gate = acc[:, wide : wide + dcols]
    dense_hidden[...] = (
        gate * jax.nn.sigmoid(gate) * acc[:, wide + dcols : wide + 2 * dcols]
    ).astype(BF16)

    piece = half // CHUNKS
    step = min(256, piece)

    def branch(at):
        expert_part = jnp.dot(hidden[...], ed[:, at], preferred_element_type=F32)
        dense_part = jnp.dot(dense_hidden[...], dd[:, at], preferred_element_type=F32)
        return expert_part * opening[:, :1] + dense_part * opening[:, LANES : LANES + 1]

    def swap(c):
        return remote(other.at[c], other_in.at[c], sws.at[c], swr.at[c], me, mate)

    for c in range(CHUNKS):

        @pl.loop(0, piece // step)
        def _(j, c=c):
            src = pl.ds(pl.multiple_of(mate * half + c * piece + j * step, step), step)
            other[c, :, pl.ds(pl.multiple_of(j * step, step), step)] = branch(src).astype(BF16)

        swap(c).start()

    def in_group(c, z, k, source):
        peer = lax.rem(i + k, INNER)
        return remote(
            summed.at[c, z, peer], plane_in.at[c, z, source], f1s.at[c, z, k], f1r.at[c, z, k],
            o * INNER + peer, tp,
        )

    def in_line(c, k, source):
        peer = lax.rem(o + k, outer)
        return remote(
            line_out.at[c, peer], line_in.at[c, source], f2s.at[c, k], f2r.at[c, k],
            peer * INNER + i, tp,
        )

    for c in range(CHUNKS):
        swap(c).wait()

        @pl.loop(0, piece // step)
        def _(j, c=c):
            src = pl.ds(pl.multiple_of(tp * half + c * piece + j * step, step), step)
            at = pl.ds(pl.multiple_of(j * step, step), step)
            both = branch(src) + other_in[c, :, at].astype(F32)
            summed[c, :, :, :, at] = both.astype(BF16).reshape(outer, INNER, seqs, step)

        @pl.loop(1, outer + 1)
        def _(k, c=c):
            z = lax.rem(o + k, outer)
            for j in range(1, INNER):
                in_group(c, z, j, i).start()

    for c in range(CHUNKS):

        @pl.loop(1, outer + 1)
        def _(k, c=c):
            z = lax.rem(o + k, outer)
            got = summed[c, z, i].astype(F32)
            for j in range(1, INNER):
                copy = in_group(c, z, j, lax.rem(i + INNER - j, INNER))
                copy.wait_send()
                copy.wait_recv()
                got = got + plane_in[c, z, lax.rem(i + INNER - j, INNER)].astype(F32)

            line_out[c, z] = got.astype(BF16)

            @pl.when(k < outer)
            def _():
                in_line(c, k, o).start()

    for c in range(CHUNKS):
        line_in[c, o] = line_out[c, o]

        @pl.loop(1, outer)
        def _(k, c=c):
            copy = in_line(c, k, lax.rem(o + outer - k, outer))
            copy.wait_send()
            copy.wait_recv()

        got = lax.fori_loop(
            0, outer, lambda z, carry, c=c: carry + line_in[c, z].astype(F32),
            jnp.zeros((seqs, piece), F32),
        )
        kept_row = row[:, pl.ds(pl.multiple_of(tp * half + c * piece, piece), piece)]
        final[:, c * piece : (c + 1) * piece] = (kept_row + got).astype(BF16)

    last = remote(final, final_in, fs, fr, me, mate)
    last.start()
    out_ref[:, pl.ds(pl.multiple_of(tp * half, half), half)] = final[...]
    last.wait()
    out_ref[:, pl.ds(pl.multiple_of(mate * half, half), half)] = final_in[...]


def layer(n, args):
    x, pos, freq, ids, weight, nmix, nffn, opened, gain, state = args[:10]
    wq, wout, eg, ed, dg, dd = args[10], args[14], args[15], args[17], args[18], args[20]
    seqs, width = x.shape
    heads, dim = state.shape[1], state.shape[2]
    hw, block, half, tokens = heads * dim, width // n, width // 2, n * seqs
    outer = n // INNER
    span, group, kb, piece = INNER // 2, INNER * seqs, INNER * block, half // CHUNKS
    slabs = hw // WIDE
    cols, dcols = eg.shape[2], dg.shape[1]
    vm, sem = pltpu.VMEM, pltpu.SemaphoreType.DMA
    vmem = pl.BlockSpec(memory_space=pltpu.VMEM)
    hbm = pl.BlockSpec(memory_space=pltpu.HBM)
    return pl.pallas_call(
        functools.partial(layer_kernel, n, heads, dim),
        out_shape=(
            jax.ShapeDtypeStruct((seqs, width), BF16),
            jax.ShapeDtypeStruct((seqs, hw), F32),
            jax.ShapeDtypeStruct((seqs, hw), BF16),
        ),
        in_specs=[hbm] * len(args),
        out_specs=(vmem, vmem, vmem),
        scratch_shapes=[
            vm(x.shape, BF16), pltpu.SMEM(pos.shape, jnp.int32), vm(freq.shape, F32),
            vm(ids.shape, jnp.int32), vm(weight.shape, BF16), vm(nmix.shape, BF16),
            vm(nffn.shape, BF16), vm(opened.shape, BF16), vm(gain.shape, BF16),
            vm(state.shape, F32), vm(eg.shape[1:], BF16), vm(eg.shape[1:], BF16),
            vm(ed.shape[1:], BF16), vm(dg.shape, BF16), vm(dg.shape, BF16), vm(dd.shape, BF16),
            vm((outer, 2, seqs, kb // 2), BF16),
            vm((2, n, seqs, kb // 2), BF16),
            vm((PIECES * seqs, seqs * dim), BF16),
            vm((slabs, INNER, block, WIDE), BF16),
            vm((2, span, hw, block), BF16),
            vm((2, hw, span * block), BF16),
            vm((slabs, outer, group, WIDE), BF16),
            vm((slabs, outer, group, WIDE), BF16),
            vm((slabs, INNER, seqs, WIDE), BF16),
            vm((slabs, INNER, seqs, WIDE), BF16),
            vm((1, hw), F32),
            vm((LANES, LANES), F32),
            vm((n, 1, LANES), F32),
            vm((n, 1, LANES), F32),
            vm((seqs, dim), F32), vm((seqs, dim), F32), vm((seqs, dim), F32),
            vm((slabs, seqs, WIDE), BF16),
            vm((slabs, 2 * outer, seqs, WIDE), BF16),
            vm((outer, seqs, span * block), BF16),
            vm((2 * outer, seqs, span * block), BF16),
            vm((seqs, width), F32),
            vm((2, seqs, half), BF16),
            vm((2, n, seqs, half), BF16),
            vm((LANES, width), BF16),
            vm((tokens, 2 * cols + 2 * dcols + LANES), F32),
            vm((tokens, cols), BF16),
            vm((tokens, dcols), BF16),
            vm((tokens, 2 * LANES), F32),
            vm((CHUNKS, tokens, piece), BF16),
            vm((CHUNKS, tokens, piece), BF16),
            vm((CHUNKS, outer, INNER, seqs, piece), BF16),
            vm((CHUNKS, outer, INNER, seqs, piece), BF16),
            vm((CHUNKS, outer, seqs, piece), BF16),
            vm((CHUNKS, outer, seqs, piece), BF16),
            vm((seqs, half), BF16),
            vm((seqs, half), BF16),
            sem((16,)),
            sem((n,)), sem((n,)), sem((2,)),
            sem((slabs, INNER)), sem((slabs, INNER)), sem((slabs + 1,)),
            sem((INNER,)), sem((2, span)),
            sem((n,)), sem((n,)),
            sem((slabs, outer)), sem((slabs, outer)),
            sem((slabs, INNER)), sem((slabs, INNER)),
            sem((slabs, 2 * outer)), sem((slabs, 2 * outer)),
            sem((2 * outer,)), sem((2 * outer,)),
            sem((outer,)), sem((outer, INNER)), sem((n,)),
            sem((n,)), sem((n,)),
            sem((CHUNKS,)), sem((CHUNKS,)),
            sem((CHUNKS, outer, INNER)), sem((CHUNKS, outer, INNER)),
            sem((CHUNKS, outer)), sem((CHUNKS, outer)),
            sem, sem,
        ],
        compiler_params=pltpu.CompilerParams(
            collective_id=0, has_side_effects=True, vmem_limit_bytes=60 * 2**20
        ),
        name="layer",
    )(*args)


def update_kernel(heads, out_in, key_ref, value_ref, state_ref, out_ref, new_ref):
    seqs = key_ref.shape[0]
    dim = value_ref.shape[1] // heads
    tp = lax.axis_index("tp")

    @pl.when(pl.program_id(0) == 0)
    def _():
        out_ref[...] = out_in[...]

    row = lax.broadcasted_iota(jnp.int32, (seqs, 2 * dim), 0)
    lane = lax.broadcasted_iota(jnp.int32, (seqs, 2 * dim), 1) // dim
    for h in range(heads):
        gamma = jnp.where(tp == 0, F32(decay(h, HEADS)), F32(decay(heads + h, HEADS)))
        at = slice(h * dim, (h + 1) * dim)
        key = split(key_ref[:, at]).T.astype(BF16)
        value = value_ref[:, at].astype(F32)
        twice = jnp.concatenate([value, value], axis=1)
        for s in range(0, seqs, 2):
            spread = jnp.where(row == s + lane, twice, 0.0)
            spread = jnp.concatenate([spread] * PIECES, axis=0).astype(BF16)
            added = jnp.dot(key, spread, preferred_element_type=F32)
            for t in range(2):
                new_ref[s + t, h] = gamma * state_ref[s + t, h] + added[:, t * dim : (t + 1) * dim]


def update(out, key, value, state):
    seqs, heads, dim = state.shape[:3]
    few = min(8, seqs)
    held = pl.BlockSpec((few, heads, dim, dim), lambda j: (j, 0, 0, 0))
    piece = pl.BlockSpec((few, heads * dim), lambda j: (j, 0))
    whole = pl.BlockSpec(out.shape, lambda j: (0, 0))
    return pl.pallas_call(
        functools.partial(update_kernel, heads),
        grid=(seqs // few,),
        out_shape=(
            jax.ShapeDtypeStruct(out.shape, BF16),
            jax.ShapeDtypeStruct(state.shape, F32),
        ),
        in_specs=[whole, piece, piece, held],
        out_specs=(whole, held),
        compiler_params=pltpu.CompilerParams(vmem_limit_bytes=60 * 2**20),
        name="update",
    )(out, key, value, state)


def on_device(
    inputs,
    positions,
    ret_state,
    norm_mix,
    w_query,
    w_key,
    w_value,
    w_gate_in,
    head_gain,
    w_out,
    norm_ffn,
    route_ids,
    route_weight,
    exp_gate,
    exp_up,
    exp_down,
    dense_gate,
    dense_up,
    dense_down,
    branch_gate,
):
    n = lax.axis_size("ep")
    dim = ret_state.shape[2]
    assert exp_gate.shape[0] == 1 and n % (2 * INNER) == 0 and n <= LANES
    assert w_query.shape[1] % WIDE == 0 and WIDE % dim == 0
    turns = 10000.0 ** (-2.0 * np.arange(dim // 2) / dim)
    freq = jnp.asarray(np.concatenate([turns, turns])[None].astype(np.float32))
    out, key, value = layer(
        n,
        (inputs, positions, freq, route_ids.T, route_weight.T, norm_mix, norm_ffn, branch_gate,
         head_gain, ret_state, w_query, w_key, w_value, w_gate_in, w_out, exp_gate, exp_up,
         exp_down, dense_gate, dense_up, dense_down),
    )
    return update(out, key, value, ret_state)


def solution(mesh):
    in_specs = (
        P("ep", None),
        P("ep"),
        P("ep", "tp", None, None),
        P(),
        P("ep", "tp"),
        P("ep", "tp"),
        P("ep", "tp"),
        P("ep", "tp"),
        P("tp"),
        P("tp", "ep"),
        P(),
        P("ep", None),
        P("ep", None),
        P("ep", None, "tp"),
        P("ep", None, "tp"),
        P("ep", "tp", None),
        P(None, ("ep", "tp")),
        P(None, ("ep", "tp")),
        P(("ep", "tp"), None),
        P(),
    )
    out_specs = (P("ep", None), P("ep", "tp", None, None))
    return jax.shard_map(
        on_device, mesh=mesh, in_specs=in_specs, out_specs=out_specs, check_vma=False
    )
```

time: 110 us -> 79.1 us (0.72)
  local copies, waits for them, and re-layouts: 19.1 us -> 0 us
  Pallas kernels: 89.4 us -> 78.3 us
    unnamed x44 -> x0, local copies, waits for them, and re-layouts: 19.1 us -> none
    pallas_call x1, Pallas kernels: 84.2 us -> 73 us  [layer(): pl.pallas_call(functools.partial(layer_kernel, n, heads, dim), out_shape=...]
where the time goes in v2:
time: 79.1 us; the launch traced here: 78.9 us
  Pallas kernels  78.3 us (99%)
    pallas_call x1, Pallas kernels, layer(): pl.pallas_call(functools.partial(layer_kernel, n, heads, dim), out_shape=...  73 us
    pallas_call x1, Pallas kernels, update(): pl.pallas_call(functools.partial(update_kernel, heads), grid=(seqs // few...  5.29 us

profile of v2, /device:TPU:0, one launch (start us, length us, event | category | flops | bytes accessed | tf_op | source)
XLA Modules:
  0.0 78.9 jit_solution(9094885892827536332)
XLA Ops:
  0.6 73.0 %layer.1 = (bf16[16,2048]{1,0:T(8,128)(2,1)}, f32[16,768]{1,0:T(8,128)}, bf16[16,768]{1,0:T(8,128)(2,1)}) custom-call(bf16[16,2048]{1,0:T(8,128)(2,1)} %x_hbm.1, s32[16]{0:T(128)} %pos_hbm.1, f32[1,128]{1,0:T(1,128)} %constant.2.clone.freq_hbm, s32[4,16]{1,0:T(4,128)} %bitcast.2, bf16[4,16]{1,0:T(4,128)(2,1)} %bitcast.3, bf16[2048]{0:T(1024)(128)(2,1)} %nmix_hbm.1, ...), custom_call_target="tpu_custom_call" | custom-call | tf_op jit(solution)/shard_map/layer/pallas_call | solution.py:679
  73.6 5.3 %update.1 = (bf16[16,2048]{1,0:T(8,128)(2,1)}, f32[16,6,128,128]{3,2,1,0:T(8,128)}) custom-call(bf16[16,2048]{1,0:T(8,128)(2,1)} %get-tuple-element.5.out_in, f32[16,768]{1,0:T(8,128)} %get-tuple-element.6.key_ref, bf16[16,768]{1,0:T(8,128)(2,1)} %get-tuple-element.7.value_ref, f32[16,6,128,128]{3,2,1,0:T(8,128)} %state_ref.1), custom_call_target="tpu_custom_call" | custom-call | tf_op jit(solution)/shard_map/update/pallas_call | solution.py:783

commit v3 on v2

--- a/solution.py
+++ b/solution.py
@@ -17,7 +17,7 @@
 BF16 = jnp.bfloat16
 INNER = 4
 CHUNKS = 2
-WIDE = 256
+WIDE = 384
 PIECES = 3
 
 
@@ -57,11 +57,11 @@
     out_ref, key_ref, value_ref,
     x_ref, pos_ref, freq_ref, ids_ref, weight_ref, nmix_ref, nffn_ref, open_ref, gain_ref,
     state, eg, eu, ed, dg, du, dd,
-    xsend, xrows, spread, wcol, wo, wo_flat, parts, zin, zsum, qkvg,
+    xsend, xrows, spread, wcol, wo, wo_flat, parts, zin, qkvg,
     gain_wide, table, share_rows, shares, cos_ref, sin_ref, readout, kept, heads_in,
-    mixs, mixin, row, half_out, gathered, open_rows, acc, hidden, dense_hidden, opening,
-    other, other_in, summed, plane_in, line_out, line_in, final, final_in,
-    load, xs, xr, xm, ws, wr, local, outs, outr, shs, shr, zs, zr, ps, pr, cs, cr, ds, dr,
+    raw, xline, rblock, row, gathered, nffn_wide, open_rows, squares, scales, acc, hidden, dense_hidden, opening,
+    other, other_in, own, summed, plane_in, line_out, line_in, final, final_in,
+    load, xs, xr, xm, ws, wr, local, outs, outr, shs, shr, zs, zr, cs, cr, xls, xlr,
     ezs, eps, er, ms, mr, sws, swr, f1s, f1r, f2s, f2r, fs, fr,
 ):
     me, tp = lax.axis_index("ep"), lax.axis_index("tp")
@@ -93,6 +93,14 @@
     for copy in small:
         copy.start()
 
+    def on_line(far, act):
+        for sign in (1, -1):
+            peer = o + sign * far
+
+            @pl.when(jnp.logical_and(peer >= 0, peer < outer))
+            def _(peer=peer):
+                act(peer)
+
     barrier = pltpu.get_barrier_semaphore()
 
     def greet(ep, core):
@@ -114,7 +122,9 @@
     normed = normalize(x_ref[...].astype(F32), nmix_ref[...].astype(F32).reshape(1, width))
     for z in range(outer):
         for c in range(2):
-            xsend[z, c] = normed[:, z * kb + c * (kb // 2) : z * kb + (c + 1) * (kb // 2)]
+            at = slice(z * kb + c * (kb // 2), z * kb + (c + 1) * (kb // 2))
+            xsend[z, c] = normed[:, at]
+            raw[z, c] = x_ref[:, at]
     pl.semaphore_wait(barrier, n - 1 + INNER + outer - 1)
 
     @pl.loop(1, n)
@@ -155,17 +165,17 @@
     own_wout = pltpu.make_async_copy(wout_hbm, wo.at[tp, slot], local.at[slabs])
     mate_wout = remote(wout_hbm, wo.at[tp, slot], outs.at[0], outr.at[tp, slot], me, mate)
 
-    for k in range(1, INNER):
-        block_to(k).start()
-
-    @pl.when(holder == tp)
-    def _():
-        own_wout.start()
-
-    @pl.when(holder != tp)
-    def _():
-        mate_wout.start()
-
+    def columns_to(k, source):
+        peer = lax.rem(o + k, outer)
+        return remote(
+            raw.at[peer, tp], xline.at[source], xls.at[k], xlr.at[k], peer * INNER + i, tp
+        )
+
+    @pl.loop(1, outer)
+    def _(k):
+        columns_to(k, o).start()
+
+    xline[o] = raw[o, tp]
     for copy in large:
         copy.start()
     xrows[tp, me] = xsend[o, tp]
@@ -202,8 +212,13 @@
     cos_ref[...] = jnp.cos(angles)
     sine = jnp.sin(angles)
     sin_ref[...] = jnp.where(lower, -sine, sine)
-    open_rows[...] = jnp.broadcast_to(open_ref[...].astype(F32).reshape(1, width), open_rows.shape).astype(BF16)
-
+    gains = nffn_ref[...].astype(F32).reshape(1, width)
+    opens = open_ref[...].astype(F32).reshape(1, width)
+    for z in range(outer):
+        for c in range(2):
+            at = slice(z * kb + c * (kb // 2), z * kb + (c + 1) * (kb // 2))
+            nffn_wide[z, c] = gains[:, at]
+            open_rows[z, c] = jnp.broadcast_to(opens[:, at], (LANES, kb // 2)).astype(BF16)
     apart = lax.rem(lax.broadcasted_iota(jnp.int32, spread.shape, 0), seqs)
     spread[...] = jnp.where(
         apart == lax.broadcasted_iota(jnp.int32, spread.shape, 1) // dim, 1.0, 0.0
@@ -224,11 +239,22 @@
 
     rows_to_mate(tp).start()
 
-    def to_line(c, k, source):
-        peer = lax.rem(o + k, outer)
+    def to_owner(c, peer, source):
         return remote(
-            parts.at[c, peer], zin.at[c, source], zs.at[c, k], zr.at[c, k], peer * INNER + i, tp
-        )
+            parts.at[c, peer], zin.at[c, source], zs.at[c, peer], zr.at[c, source], peer, tp
+        )
+
+    def scatter(c):
+        @pl.loop(1, outer)
+        def _(d):
+            def send(z):
+                for j in range(INNER):
+                    to_owner(c, z * INNER + j, me).start()
+
+            on_line(outer - d, send)
+
+        for k in range(1, INNER):
+            to_owner(c, o * INNER + lax.rem(i + k, INNER), me).start()
 
     for c in range(slabs):
         for m, w in enumerate((wq, wk, wv, wg)):
@@ -255,17 +281,19 @@
             )
             for q in range(2)
         )
-        parts[c] = product.astype(BF16).reshape(outer, group, WIDE)
-
-        @pl.loop(1, outer)
-        def _(k, c=c):
-            to_line(c, k, o).start()
-
-    def to_plane(c, k, source):
-        peer = lax.rem(i + k, INNER)
-        return remote(
-            zsum.at[c, peer], qkvg.at[c, source], ps.at[c, k], pr.at[c, k], o * INNER + peer, tp
-        )
+        parts[c] = product.astype(BF16).reshape(n, seqs, WIDE)
+        scatter(c)
+
+    for k in range(1, INNER):
+        block_to(k).start()
+
+    @pl.when(holder == tp)
+    def _():
+        own_wout.start()
+
+    @pl.when(holder != tp)
+    def _():
+        mate_wout.start()
 
     def head(c, q):
         h = c * per_slab + q
@@ -312,10 +340,17 @@
         return to_cores(lambda p: kept.at[c], heads_in.at[c, source], cs.at[c], cr.at[c], j)
 
     def retain(c):
-        for k in range(1, INNER):
-            copy = to_plane(c, k, lax.rem(i + INNER - k, INNER))
+        zin[c, me] = parts[c, me]
+
+        @pl.loop(1, n)
+        def _(k):
+            came = lax.rem(me + k, n)
+            copy = to_owner(c, came, came)
             copy.wait_send()
             copy.wait_recv()
+
+        for m in range(INNER):
+            qkvg[c, m] = sum(zin[c, z * INNER + m].astype(F32) for z in range(outer)).astype(BF16)
         for q in range(per_slab):
             head(c, q)
 
@@ -327,25 +362,7 @@
 
     large[0].wait()
     for c in range(slabs):
-
-        @pl.loop(1, outer)
-        def _(k, c=c):
-            copy = to_line(c, k, lax.rem(o + outer - k, outer))
-            copy.wait_send()
-            copy.wait_recv()
-
-        zin[c, o] = parts[c, o]
-        total = lax.fori_loop(
-            0, outer, lambda z, carry, c=c: carry + zin[c, z].astype(F32),
-            jnp.zeros((group, WIDE), F32),
-        )
-        zsum[c] = total.astype(BF16).reshape(INNER, seqs, WIDE)
-        for k in range(1, INNER):
-            to_plane(c, k, i).start()
-        qkvg[c, i] = zsum[c, i]
-        if c > 0:
-            retain(c - 1)
-    retain(slabs - 1)
+        retain(c)
 
     for k in range(1, INNER):
         block_to(k).wait_send()
@@ -388,40 +405,21 @@
         ).astype(BF16)
         for q in range(2)
     )
-    mixs[...] = (first.astype(F32) + second.astype(F32)).astype(BF16).reshape(
-        outer, seqs, span * block
-    )
-
-    def mixed_to(j, source):
-        return to_cores(lambda p: mixs.at[p], mixin.at[source], ds, dr, j)
-
-    @pl.loop(1, 2 * outer)
-    def _(j):
-        mixed_to(j, mine).start()
-
-    mixin[mine] = mixs[o]
-    @pl.loop(1, 2 * outer)
-    def _(j):
-        copy = mixed_to(j, source_of(j))
+    mixer = (first.astype(F32) + second.astype(F32)).astype(BF16).astype(F32)
+
+    @pl.loop(1, outer)
+    def _(k):
+        copy = columns_to(k, lax.rem(o + outer - k, outer))
         copy.wait_send()
         copy.wait_recv()
 
-    for z in range(outer):
-        for j in range(INNER):
-            b = z * INNER + j
-            row[:, b * block : (b + 1) * block] = mixin[
-                (j // span) * outer + z, :, (j % span) * block : (j % span + 1) * block
-            ].astype(F32)
-    residual = (x_ref[...].astype(F32) + row[...]).astype(BF16).astype(F32)
-    row[...] = residual
-    normed = normalize(residual, nffn_ref[...].astype(F32).reshape(1, width))
-    for c in range(2):
-        half_out[c] = normed[:, c * half : (c + 1) * half]
+    residual = (xline[...].reshape(outer * seqs, kb // 2).astype(F32) + mixer).astype(BF16)
+    rblock[...] = residual
+    gathered[tp, me] = residual
 
     def along(peer, block_id):
         return remote(
-            half_out.at[tp], gathered.at[tp, block_id], ezs.at[peer], er.at[block_id],
-            peer * INNER + i, tp,
+            rblock, gathered.at[tp, block_id], ezs.at[peer], er.at[block_id], peer * INNER + i, tp
         )
 
     def inside(src, k, z, block_id):
@@ -430,121 +428,31 @@
             src, gathered.at[tp, block_id], eps.at[z, k], er.at[block_id], o * INNER + peer, tp
         )
 
-    def across_cores(half_id, block_id):
+    def across_cores(src, half_id, block_id):
         return remote(
-            gathered.at[tp, block_id], gathered.at[half_id, block_id], ms.at[block_id],
-            mr.at[block_id], me, mate,
-        )
-
-    def on_line(far, act):
-        for sign in (1, -1):
-            peer = o + sign * far
-
-            @pl.when(jnp.logical_and(peer >= 0, peer < outer))
-            def _(peer=peer):
-                act(peer)
+            src, gathered.at[half_id, block_id], ms.at[block_id], mr.at[block_id], me, mate
+        )
 
     @pl.loop(1, outer)
     def _(d):
         on_line(outer - d, lambda peer: along(peer, me).start())
 
     for k in range(1, INNER):
-        inside(half_out.at[tp], k, o, me).start()
-    for c in range(2):
-        gathered[c, me] = half_out[c]
+        inside(rblock, k, o, me).start()
+    across_cores(rblock, tp, me).start()
 
     def from_group(z):
         for j in range(1, INNER):
             came = z * INNER + lax.rem(i + INNER - j, INNER)
-            inside(half_out.at[tp], j, z, came).wait_recv()
-            across_cores(tp, came).start()
+            inside(rblock, j, z, came).wait_recv()
+            across_cores(gathered.at[tp, came], tp, came).start()
 
     def relay(peer):
         came = peer * INNER + i
         along(peer, came).wait_recv()
         for j in range(1, INNER):
             inside(gathered.at[tp, came], j, peer, came).start()
-        across_cores(tp, came).start()
-
-    cols = eg.shape[1]
-    dcols = dg.shape[1]
-    tile = min(256, cols)
-    wide = 2 * cols
-    part_rows = tokens // 2
-    near = o // (outer // 2)
-
-    def half_dot(g, c, first):
-        per = n // 2
-        left = gathered[c, pl.ds(g * per, per)].reshape(part_rows, half)
-        k_at = pl.ds(pl.multiple_of(c * half, half), half)
-        rows = pl.ds(pl.multiple_of(g * part_rows, part_rows), part_rows)
-
-        def put(at, value):
-            if first:
-                acc[rows, at] = value
-            else:
-                acc[rows, at] += value
-
-        for base, w in ((0, eg), (cols, eu)):
-
-            @pl.loop(0, cols // tile)
-            def _(j, base=base, w=w):
-                src = pl.ds(pl.multiple_of(j * tile, tile), tile)
-                dst = pl.ds(pl.multiple_of(base + j * tile, tile), tile)
-                put(dst, jnp.dot(left, w[k_at, src], preferred_element_type=F32))
-
-        for base, w in ((wide, dg), (wide + dcols, du)):
-            put(slice(base, base + dcols), jnp.dot(left, w[k_at, :], preferred_element_type=F32))
-        put(
-            slice(wide + 2 * dcols, wide + 2 * dcols + LANES),
-            lax.dot_general(
-                left, open_rows[:, k_at], (((1,), (1,)), ((), ())), preferred_element_type=F32
-            ),
-        )
-
-    def from_mate(g):
-        @pl.loop(0, n // 2)
-        def _(q):
-            block_id = g * (n // 2) + q
-
-            @pl.when(block_id != me)
-            def _():
-                copy = across_cores(mate, block_id)
-                copy.wait_send()
-                copy.wait_recv()
-
-    @pl.loop(1, outer)
-    def _(d):
-        on_line(d, relay)
-
-    @pl.loop(0, outer // 2)
-    def _(z):
-        from_group(near * (outer // 2) + z)
-
-    for copy in large[1:]:
-        copy.wait()
-
-    half_dot(near, tp, True)
-    from_mate(near)
-    half_dot(near, mate, False)
-    away = 1 - near
-
-    @pl.loop(0, outer // 2)
-    def _(z):
-        from_group(away * (outer // 2) + z)
-
-    half_dot(away, tp, True)
-    from_mate(away)
-    half_dot(away, mate, False)
-
-    @pl.loop(1, outer)
-    def _(d):
-        on_line(d, lambda peer: along(peer, me).wait_send())
-
-    @pl.loop(0, outer)
-    def _(z):
-        for j in range(1, INNER):
-            inside(half_out.at[tp], j, z, me).wait_send()
+        across_cores(gathered.at[tp, came], tp, came).start()
 
     @pl.loop(1, n)
     def _(k):
@@ -556,20 +464,93 @@
         table[j : j + 1, :] = shares[j]
     columns = table[...].T[:seqs]
     for j in range(n):
-        opening[j * seqs : (j + 1) * seqs, :LANES] = jnp.broadcast_to(
-            columns[:, j : j + 1], (seqs, LANES)
-        )
-    opening[:, LANES:] = jax.nn.sigmoid(acc[:, wide + 2 * dcols : wide + 2 * dcols + LANES])
+        at = ((j % INNER) * outer + j // INNER) * seqs
+        opening[at : at + seqs, :LANES] = jnp.broadcast_to(columns[:, j : j + 1], (seqs, LANES))
+
+    cols = eg.shape[1]
+    dcols = dg.shape[1]
+    tile = min(256, cols)
+    wide = 2 * cols
+
+    def chunk(z, c, first):
+        got = gathered[c, pl.ds(z * INNER, INNER)].reshape(tokens, kb // 2).astype(F32)
+        left = (got * nffn_wide[z, c]).astype(BF16)
+        k_at = pl.ds(pl.multiple_of(z * kb + c * (kb // 2), kb // 2), kb // 2)
+
+        def put(ref, at, value):
+            if first:
+                ref[:, at] = value
+            else:
+                ref[:, at] += value
+
+        put(squares, slice(None), got * got)
+        for base, w in ((0, eg), (cols, eu)):
+            for j in range(cols // tile):
+                src = slice(j * tile, (j + 1) * tile)
+                dst = slice(base + j * tile, base + (j + 1) * tile)
+                put(acc, dst, jnp.dot(left, w[k_at, src], preferred_element_type=F32))
+        for base, w in ((wide, dg), (wide + dcols, du)):
+            put(
+                acc, slice(base, base + dcols),
+                jnp.dot(left, w[k_at, :], preferred_element_type=F32),
+            )
+        put(
+            acc, slice(wide + 2 * dcols, wide + 2 * dcols + LANES),
+            lax.dot_general(
+                left, open_rows[z, c], (((1,), (1,)), ((), ())), preferred_element_type=F32
+            ),
+        )
+
+    def from_mate(z):
+        for j in range(INNER):
+            copy = across_cores(rblock, mate, z * INNER + j)
+            copy.wait_send()
+            copy.wait_recv()
+
+    def own_part(z):
+        from_group(z)
+        chunk(z, tp, False)
+
+    def mate_part(z):
+        from_mate(z)
+        chunk(z, mate, False)
+
+    @pl.loop(1, outer)
+    def _(d):
+        on_line(d, relay)
+
+    for copy in large[1:]:
+        copy.wait()
+
+    from_group(o)
+    chunk(o, tp, True)
+    on_line(1, own_part)
+    mate_part(o)
+
+    @pl.loop(2, outer)
+    def _(d):
+        on_line(d, own_part)
+        on_line(d - 1, mate_part)
+
+    on_line(outer - 1, mate_part)
+
+    mean = jnp.sum(squares[...], axis=-1, keepdims=True) * (1.0 / width)
+    scales[...] = jnp.broadcast_to(lax.rsqrt(mean + EPS), (tokens, LANES))
+    opening[:, LANES:] = jax.nn.sigmoid(
+        scales[...] * acc[:, wide + 2 * dcols : wide + 2 * dcols + LANES]
+    )
+    scale = scales[:, :1]
 
     @pl.loop(0, cols // tile)
     def _(j):
         at = pl.ds(pl.multiple_of(j * tile, tile), tile)
-        gate, up = acc[:, at], acc[:, pl.ds(pl.multiple_of(cols + j * tile, tile), tile)]
+        gate = scale * acc[:, at]
+        up = scale * acc[:, pl.ds(pl.multiple_of(cols + j * tile, tile), tile)]
         hidden[:, at] = (gate * jax.nn.sigmoid(gate) * up).astype(BF16)
 
-    gate = acc[:, wide : wide + dcols]
+    gate = scale * acc[:, wide : wide + dcols]
     dense_hidden[...] = (
-        gate * jax.nn.sigmoid(gate) * acc[:, wide + dcols : wide + 2 * dcols]
+        gate * jax.nn.sigmoid(gate) * (scale * acc[:, wide + dcols : wide + 2 * dcols])
     ).astype(BF16)
 
     piece = half // CHUNKS
@@ -595,57 +576,82 @@
     def in_group(c, z, k, source):
         peer = lax.rem(i + k, INNER)
         return remote(
-            summed.at[c, z, peer], plane_in.at[c, z, source], f1s.at[c, z, k], f1r.at[c, z, k],
+            summed.at[c, peer, z], plane_in.at[c, z, source], f1s.at[c, z, k], f1r.at[c, z, k],
             o * INNER + peer, tp,
         )
 
-    def in_line(c, k, source):
-        peer = lax.rem(o + k, outer)
+    def in_line(c, peer, source):
         return remote(
-            line_out.at[c, peer], line_in.at[c, source], f2s.at[c, k], f2r.at[c, k],
+            line_out.at[c, peer], line_in.at[c, source], f2s.at[c, peer], f2r.at[c, source],
             peer * INNER + i, tp,
         )
 
+    def send_group(c, z):
+        for j in range(1, INNER):
+            in_group(c, z, j, i).start()
+
     for c in range(CHUNKS):
+        mine_at = pl.multiple_of(tp * half + c * piece, piece)
+        for j in range(piece // step):
+            own[:, j * step : (j + 1) * step] = branch(pl.ds(mine_at + j * step, step))
         swap(c).wait()
-
-        @pl.loop(0, piece // step)
-        def _(j, c=c):
-            src = pl.ds(pl.multiple_of(tp * half + c * piece + j * step, step), step)
-            at = pl.ds(pl.multiple_of(j * step, step), step)
-            both = branch(src) + other_in[c, :, at].astype(F32)
-            summed[c, :, :, :, at] = both.astype(BF16).reshape(outer, INNER, seqs, step)
-
-        @pl.loop(1, outer + 1)
-        def _(k, c=c):
-            z = lax.rem(o + k, outer)
-            for j in range(1, INNER):
-                in_group(c, z, j, i).start()
+        for j in range(piece // step):
+            at = slice(j * step, (j + 1) * step)
+            both = own[:, at] + other_in[c, :, at].astype(F32)
+            summed[c, :, :, :, at] = both.astype(BF16).reshape(INNER, outer, seqs, step)
+
+        @pl.loop(1, outer)
+        def _(d, c=c):
+            on_line(outer - d, functools.partial(send_group, c))
 
     for c in range(CHUNKS):
-
-        @pl.loop(1, outer + 1)
-        def _(k, c=c):
-            z = lax.rem(o + k, outer)
-            got = summed[c, z, i].astype(F32)
-            for j in range(1, INNER):
-                copy = in_group(c, z, j, lax.rem(i + INNER - j, INNER))
-                copy.wait_send()
-                copy.wait_recv()
-                got = got + plane_in[c, z, lax.rem(i + INNER - j, INNER)].astype(F32)
-
-            line_out[c, z] = got.astype(BF16)
-
-            @pl.when(k < outer)
-            def _():
-                in_line(c, k, o).start()
+        send_group(c, o)
+
+    @pl.loop(1, outer)
+    def _(d):
+        on_line(d, lambda peer: along(peer, me).wait_send())
+
+    @pl.loop(0, outer)
+    def _(z):
+        for j in range(1, INNER):
+            inside(rblock, j, z, me).wait_send()
+
+    for z in range(outer):
+        for c in range(2):
+            row[:, z * kb + c * (kb // 2) : z * kb + (c + 1) * (kb // 2)] = gathered[
+                c, z * INNER + i, pl.ds(pl.multiple_of(o * seqs, seqs), seqs), :
+            ].astype(F32)
+
+    def reduce_group(c, z):
+        got = summed[c, i, z].astype(F32)
+        for j in range(1, INNER):
+            source = lax.rem(i + INNER - j, INNER)
+            copy = in_group(c, z, j, source)
+            copy.wait_send()
+            copy.wait_recv()
+            got = got + plane_in[c, z, source].astype(F32)
+        line_out[c, z] = got.astype(BF16)
+
+    def reduce_far(c, z):
+        reduce_group(c, z)
+        in_line(c, z, o).start()
+
+    for c in range(CHUNKS):
+
+        @pl.loop(1, outer)
+        def _(d, c=c):
+            on_line(outer - d, functools.partial(reduce_far, c))
+
+    for c in range(CHUNKS):
+        reduce_group(c, o)
 
     for c in range(CHUNKS):
         line_in[c, o] = line_out[c, o]
 
         @pl.loop(1, outer)
         def _(k, c=c):
-            copy = in_line(c, k, lax.rem(o + outer - k, outer))
+            peer = lax.rem(o + k, outer)
+            copy = in_line(c, peer, peer)
             copy.wait_send()
             copy.wait_recv()
 
@@ -697,9 +703,8 @@
             vm((slabs, INNER, block, WIDE), BF16),
             vm((2, span, hw, block), BF16),
             vm((2, hw, span * block), BF16),
-            vm((slabs, outer, group, WIDE), BF16),
-            vm((slabs, outer, group, WIDE), BF16),
-            vm((slabs, INNER, seqs, WIDE), BF16),
+            vm((slabs, n, seqs, WIDE), BF16),
+            vm((slabs, n, seqs, WIDE), BF16),
             vm((slabs, INNER, seqs, WIDE), BF16),
             vm((1, hw), F32),
             vm((LANES, LANES), F32),
@@ -708,19 +713,23 @@
             vm((seqs, dim), F32), vm((seqs, dim), F32), vm((seqs, dim), F32),
             vm((slabs, seqs, WIDE), BF16),
             vm((slabs, 2 * outer, seqs, WIDE), BF16),
-            vm((outer, seqs, span * block), BF16),
-            vm((2 * outer, seqs, span * block), BF16),
+            vm((outer, 2, seqs, kb // 2), BF16),
+            vm((outer, seqs, kb // 2), BF16),
+            vm((outer * seqs, kb // 2), BF16),
             vm((seqs, width), F32),
-            vm((2, seqs, half), BF16),
-            vm((2, n, seqs, half), BF16),
-            vm((LANES, width), BF16),
+            vm((2, n, outer * seqs, kb // 2), BF16),
+            vm((outer, 2, 1, kb // 2), F32),
+            vm((outer, 2, LANES, kb // 2), BF16),
+            vm((tokens, kb // 2), F32),
+            vm((tokens, LANES), F32),
             vm((tokens, 2 * cols + 2 * dcols + LANES), F32),
             vm((tokens, cols), BF16),
             vm((tokens, dcols), BF16),
             vm((tokens, 2 * LANES), F32),
             vm((CHUNKS, tokens, piece), BF16),
             vm((CHUNKS, tokens, piece), BF16),
-            vm((CHUNKS, outer, INNER, seqs, piece), BF16),
+            vm((tokens, piece), F32),
+            vm((CHUNKS, INNER, outer, seqs, piece), BF16),
             vm((CHUNKS, outer, INNER, seqs, piece), BF16),
             vm((CHUNKS, outer, seqs, piece), BF16),
             vm((CHUNKS, outer, seqs, piece), BF16),
@@ -731,10 +740,9 @@
             sem((slabs, INNER)), sem((slabs, INNER)), sem((slabs + 1,)),
             sem((INNER,)), sem((2, span)),
             sem((n,)), sem((n,)),
-            sem((slabs, outer)), sem((slabs, outer)),
-            sem((slabs, INNER)), sem((slabs, INNER)),
+            sem((slabs, n)), sem((slabs, n)),
             sem((slabs, 2 * outer)), sem((slabs, 2 * outer)),
-            sem((2 * outer,)), sem((2 * outer,)),
+            sem((outer,)), sem((outer,)),
             sem((outer,)), sem((outer, INNER)), sem((n,)),
             sem((n,)), sem((n,)),
             sem((CHUNKS,)), sem((CHUNKS,)),

time: 79.1 us -> 67.1 us (0.85)
  Pallas kernels: 78.3 us -> 66.3 us
    pallas_call x1, Pallas kernels: 73 us -> 61 us  [layer(): pl.pallas_call(functools.partial(layer_kernel, n, heads, dim), out_shape=...]
where the time goes in v3:
time: 67.1 us; the launch traced here: 67 us
  Pallas kernels  66.3 us (99%)
    pallas_call x1, Pallas kernels, layer(): pl.pallas_call(functools.partial(layer_kernel, n, heads, dim), out_shape=...  61 us
    pallas_call x1, Pallas kernels, update(): pl.pallas_call(functools.partial(update_kernel, heads), grid=(seqs // few...  5.29 us

profile of v3, /device:TPU:0, one launch (start us, length us, event | category | flops | bytes accessed | tf_op | source)
XLA Modules:
  0.0 67.0 jit_solution(5677498083303346526)
XLA Ops:
  0.6 61.0 %layer.1 = (bf16[16,2048]{1,0:T(8,128)(2,1)}, f32[16,768]{1,0:T(8,128)}, bf16[16,768]{1,0:T(8,128)(2,1)}) custom-call(bf16[16,2048]{1,0:T(8,128)(2,1)} %x_hbm.1, s32[16]{0:T(128)} %pos_hbm.1, f32[1,128]{1,0:T(1,128)} %constant.2.clone.freq_hbm, s32[4,16]{1,0:T(4,128)} %bitcast.2, bf16[4,16]{1,0:T(4,128)(2,1)} %bitcast.3, bf16[2048]{0:T(1024)(128)(2,1)} %nmix_hbm.1, ...), custom_call_target="tpu_custom_call" | custom-call | tf_op jit(solution)/shard_map/layer/pallas_call | solution.py:685
  61.7 5.3 %update.1 = (bf16[16,2048]{1,0:T(8,128)(2,1)}, f32[16,6,128,128]{3,2,1,0:T(8,128)}) custom-call(bf16[16,2048]{1,0:T(8,128)(2,1)} %get-tuple-element.5.out_in, f32[16,768]{1,0:T(8,128)} %get-tuple-element.6.key_ref, bf16[16,768]{1,0:T(8,128)(2,1)} %get-tuple-element.7.value_ref, f32[16,6,128,128]{3,2,1,0:T(8,128)} %state_ref.1), custom_call_target="tpu_custom_call" | custom-call | tf_op jit(solution)/shard_map/update/pallas_call | solution.py:791

commit v4 on v3

--- a/solution.py
+++ b/solution.py
@@ -54,15 +54,15 @@
     n, heads, dim,
     x_hbm, pos_hbm, freq_hbm, ids_hbm, weight_hbm, nmix_hbm, nffn_hbm, open_hbm, gain_hbm,
     state_hbm, wq, wk, wv, wg, wout_hbm, eg_hbm, eu_hbm, ed_hbm, dg_hbm, du_hbm, dd_hbm,
-    out_ref, key_ref, value_ref,
+    packed,
     x_ref, pos_ref, freq_ref, ids_ref, weight_ref, nmix_ref, nffn_ref, open_ref, gain_ref,
     state, eg, eu, ed, dg, du, dd,
     xsend, xrows, spread, wcol, wo, wo_flat, parts, zin, qkvg,
     gain_wide, table, share_rows, shares, cos_ref, sin_ref, readout, kept, heads_in,
-    raw, xline, rblock, row, gathered, nffn_wide, open_rows, squares, scales, acc, hidden, dense_hidden, opening,
-    other, other_in, own, summed, plane_in, line_out, line_in, final, final_in,
+    raw, xline, rblock, row, gathered, nffn_wide, open_rows, squares, scales, acc, hidden, hidden_in, dense_hidden, dense_in, opening,
+    own, summed, plane_in, line_out, line_in, final, final_in,
     load, xs, xr, xm, ws, wr, local, outs, outr, shs, shr, zs, zr, cs, cr, xls, xlr,
-    ezs, eps, er, ms, mr, sws, swr, f1s, f1r, f2s, f2r, fs, fr,
+    ezs, eps, er, ms, mr, sws, swr, f1s, f1r, f2s, f2r, fs, fr, across_send, across_recv,
 ):
     me, tp = lax.axis_index("ep"), lax.axis_index("tp")
     mate = 1 - tp
@@ -75,6 +75,23 @@
     hw = heads * dim
     slabs, per_slab = hw // WIDE, WIDE // dim
 
+    def half_at(c):
+        return pl.ds(pl.multiple_of(c * half, half), half)
+
+    rows_across = [
+        remote(src, dst, across_send.at[j], across_recv.at[j], me, mate)
+        for j, (src, dst) in enumerate(
+            ((ed_hbm.at[0, :, half_at(mate)], ed.at[tp]), (dd_hbm.at[:, half_at(mate)], dd.at[tp]))
+        )
+    ]
+    rows_here = [
+        remote(src, dst, across_send.at[j], across_recv.at[j], me, mate)
+        for j, (src, dst) in enumerate(
+            ((ed_hbm.at[0, :, half_at(mate)], ed.at[mate]),
+             (dd_hbm.at[:, half_at(mate)], dd.at[mate]))
+        )
+    ]
+
     small = [
         pltpu.make_async_copy(src, dst, load.at[j])
         for j, (src, dst) in enumerate(
@@ -87,7 +104,8 @@
         pltpu.make_async_copy(src, dst, load.at[len(small) + j])
         for j, (src, dst) in enumerate(
             ((state_hbm, state), (eg_hbm.at[0], eg), (eu_hbm.at[0], eu), (dg_hbm, dg),
-             (du_hbm, du), (ed_hbm.at[0], ed), (dd_hbm, dd))
+             (du_hbm, du), (ed_hbm.at[0, :, half_at(tp)], ed.at[tp]),
+             (dd_hbm.at[:, half_at(tp)], dd.at[tp]))
         )
     ]
     for copy in small:
@@ -306,9 +324,9 @@
 
         query = rotated(0)
         key = rotated(1) * dim ** (-0.5)
-        key_ref[:, h * dim : (h + 1) * dim] = key
+        packed[:, width + h * dim : width + (h + 1) * dim] = key
         value = qkvg[c, 2, :, at].astype(F32)
-        value_ref[:, h * dim : (h + 1) * dim] = qkvg[c, 2, :, at]
+        packed[:, width + hw + h * dim : width + hw + (h + 1) * dim] = value
         across = split(query).T.astype(BF16)
         for s in range(0, seqs, 2):
             wide = jnp.dot(
@@ -363,6 +381,9 @@
     large[0].wait()
     for c in range(slabs):
         retain(c)
+
+    for copy in rows_across:
+        copy.start()
 
     for k in range(1, INNER):
         block_to(k).wait_send()
@@ -541,37 +562,46 @@
     )
     scale = scales[:, :1]
 
-    @pl.loop(0, cols // tile)
-    def _(j):
-        at = pl.ds(pl.multiple_of(j * tile, tile), tile)
-        gate = scale * acc[:, at]
-        up = scale * acc[:, pl.ds(pl.multiple_of(cols + j * tile, tile), tile)]
-        hidden[:, at] = (gate * jax.nn.sigmoid(gate) * up).astype(BF16)
+    pieces = cols // tile
+
+    def swap(src, dst, j):
+        return remote(src, dst, sws.at[j], swr.at[j], me, mate)
+
+    for j in range(pieces):
+        gate = scale * acc[:, j * tile : (j + 1) * tile]
+        up = scale * acc[:, cols + j * tile : cols + (j + 1) * tile]
+        hidden[j] = (gate * jax.nn.sigmoid(gate) * up).astype(BF16)
+        swap(hidden.at[j], hidden_in.at[j], j).start()
 
     gate = scale * acc[:, wide : wide + dcols]
     dense_hidden[...] = (
         gate * jax.nn.sigmoid(gate) * (scale * acc[:, wide + dcols : wide + 2 * dcols])
     ).astype(BF16)
+    swap(dense_hidden, dense_in, pieces).start()
 
     piece = half // CHUNKS
     step = min(256, piece)
 
-    def branch(at):
-        expert_part = jnp.dot(hidden[...], ed[:, at], preferred_element_type=F32)
-        dense_part = jnp.dot(dense_hidden[...], dd[:, at], preferred_element_type=F32)
+    def branch(units, dense_units, c, at):
+        expert_part = sum(
+            jnp.dot(
+                units[j], ed[c, j * tile : (j + 1) * tile, at], preferred_element_type=F32
+            )
+            for j in range(pieces)
+        )
+        dense_part = jnp.dot(dense_units[...], dd[c, :, at], preferred_element_type=F32)
         return expert_part * opening[:, :1] + dense_part * opening[:, LANES : LANES + 1]
 
-    def swap(c):
-        return remote(other.at[c], other_in.at[c], sws.at[c], swr.at[c], me, mate)
-
-    for c in range(CHUNKS):
-
-        @pl.loop(0, piece // step)
-        def _(j, c=c):
-            src = pl.ds(pl.multiple_of(mate * half + c * piece + j * step, step), step)
-            other[c, :, pl.ds(pl.multiple_of(j * step, step), step)] = branch(src).astype(BF16)
-
-        swap(c).start()
+    for j in range(half // step):
+        at = slice(j * step, (j + 1) * step)
+        own[:, at] = branch(hidden, dense_hidden, tp, at)
+
+    for copy in rows_here:
+        copy.wait_send()
+        copy.wait_recv()
+    for j in range(pieces):
+        swap(hidden.at[j], hidden_in.at[j], j).wait()
+    swap(dense_hidden, dense_in, pieces).wait()
 
     def in_group(c, z, k, source):
         peer = lax.rem(i + k, INNER)
@@ -591,13 +621,10 @@
             in_group(c, z, j, i).start()
 
     for c in range(CHUNKS):
-        mine_at = pl.multiple_of(tp * half + c * piece, piece)
-        for j in range(piece // step):
-            own[:, j * step : (j + 1) * step] = branch(pl.ds(mine_at + j * step, step))
-        swap(c).wait()
         for j in range(piece // step):
             at = slice(j * step, (j + 1) * step)
-            both = own[:, at] + other_in[c, :, at].astype(F32)
+            own_at = slice(c * piece + j * step, c * piece + (j + 1) * step)
+            both = own[:, own_at] + branch(hidden_in, dense_in, mate, own_at)
             summed[c, :, :, :, at] = both.astype(BF16).reshape(INNER, outer, seqs, step)
 
         @pl.loop(1, outer)
@@ -664,9 +691,9 @@
 
     last = remote(final, final_in, fs, fr, me, mate)
     last.start()
-    out_ref[:, pl.ds(pl.multiple_of(tp * half, half), half)] = final[...]
+    packed[:, pl.ds(pl.multiple_of(tp * half, half), half)] = final[...].astype(F32)
     last.wait()
-    out_ref[:, pl.ds(pl.multiple_of(mate * half, half), half)] = final_in[...]
+    packed[:, pl.ds(pl.multiple_of(mate * half, half), half)] = final_in[...].astype(F32)
 
 
 def layer(n, args):
@@ -679,24 +706,22 @@
     span, group, kb, piece = INNER // 2, INNER * seqs, INNER * block, half // CHUNKS
     slabs = hw // WIDE
     cols, dcols = eg.shape[2], dg.shape[1]
+    tile = min(256, cols)
     vm, sem = pltpu.VMEM, pltpu.SemaphoreType.DMA
     vmem = pl.BlockSpec(memory_space=pltpu.VMEM)
     hbm = pl.BlockSpec(memory_space=pltpu.HBM)
     return pl.pallas_call(
         functools.partial(layer_kernel, n, heads, dim),
-        out_shape=(
-            jax.ShapeDtypeStruct((seqs, width), BF16),
-            jax.ShapeDtypeStruct((seqs, hw), F32),
-            jax.ShapeDtypeStruct((seqs, hw), BF16),
-        ),
+        out_shape=jax.ShapeDtypeStruct((seqs, width + 2 * hw), F32),
         in_specs=[hbm] * len(args),
-        out_specs=(vmem, vmem, vmem),
+        out_specs=vmem,
         scratch_shapes=[
             vm(x.shape, BF16), pltpu.SMEM(pos.shape, jnp.int32), vm(freq.shape, F32),
             vm(ids.shape, jnp.int32), vm(weight.shape, BF16), vm(nmix.shape, BF16),
             vm(nffn.shape, BF16), vm(opened.shape, BF16), vm(gain.shape, BF16),
             vm(state.shape, F32), vm(eg.shape[1:], BF16), vm(eg.shape[1:], BF16),
-            vm(ed.shape[1:], BF16), vm(dg.shape, BF16), vm(dg.shape, BF16), vm(dd.shape, BF16),
+            vm((2, eg.shape[2], half), BF16), vm(dg.shape, BF16), vm(dg.shape, BF16),
+            vm((2, dg.shape[1], half), BF16),
             vm((outer, 2, seqs, kb // 2), BF16),
             vm((2, n, seqs, kb // 2), BF16),
             vm((PIECES * seqs, seqs * dim), BF16),
@@ -723,12 +748,12 @@
             vm((tokens, kb // 2), F32),
             vm((tokens, LANES), F32),
             vm((tokens, 2 * cols + 2 * dcols + LANES), F32),
-            vm((tokens, cols), BF16),
+            vm((cols // tile, tokens, tile), BF16),
+            vm((cols // tile, tokens, tile), BF16),
+            vm((tokens, dcols), BF16),
             vm((tokens, dcols), BF16),
             vm((tokens, 2 * LANES), F32),
-            vm((CHUNKS, tokens, piece), BF16),
-            vm((CHUNKS, tokens, piece), BF16),
-            vm((tokens, piece), F32),
+            vm((tokens, half), F32),
             vm((CHUNKS, INNER, outer, seqs, piece), BF16),
             vm((CHUNKS, outer, INNER, seqs, piece), BF16),
             vm((CHUNKS, outer, seqs, piece), BF16),
@@ -745,34 +770,31 @@
             sem((outer,)), sem((outer,)),
             sem((outer,)), sem((outer, INNER)), sem((n,)),
             sem((n,)), sem((n,)),
-            sem((CHUNKS,)), sem((CHUNKS,)),
+            sem((cols // tile + 1,)), sem((cols // tile + 1,)),
             sem((CHUNKS, outer, INNER)), sem((CHUNKS, outer, INNER)),
             sem((CHUNKS, outer)), sem((CHUNKS, outer)),
-            sem, sem,
+            sem, sem, sem((2,)), sem((2,)),
         ],
         compiler_params=pltpu.CompilerParams(
-            collective_id=0, has_side_effects=True, vmem_limit_bytes=60 * 2**20
+            collective_id=0, has_side_effects=True, vmem_limit_bytes=56 * 2**20
         ),
         name="layer",
     )(*args)
 
 
-def update_kernel(heads, out_in, key_ref, value_ref, state_ref, out_ref, new_ref):
-    seqs = key_ref.shape[0]
-    dim = value_ref.shape[1] // heads
+def update_kernel(packed, state_ref, out_ref, new_ref):
+    seqs, width = out_ref.shape
+    heads, dim = state_ref.shape[1:3]
+    hw = heads * dim
     tp = lax.axis_index("tp")
-
-    @pl.when(pl.program_id(0) == 0)
-    def _():
-        out_ref[...] = out_in[...]
-
+    out_ref[...] = packed[:, :width].astype(BF16)
     row = lax.broadcasted_iota(jnp.int32, (seqs, 2 * dim), 0)
     lane = lax.broadcasted_iota(jnp.int32, (seqs, 2 * dim), 1) // dim
     for h in range(heads):
         gamma = jnp.where(tp == 0, F32(decay(h, HEADS)), F32(decay(heads + h, HEADS)))
-        at = slice(h * dim, (h + 1) * dim)
-        key = split(key_ref[:, at]).T.astype(BF16)
-        value = value_ref[:, at].astype(F32)
+        key = packed[:, width + h * dim : width + (h + 1) * dim]
+        key = split(key).T.astype(BF16)
+        value = packed[:, width + hw + h * dim : width + hw + (h + 1) * dim]
         twice = jnp.concatenate([value, value], axis=1)
         for s in range(0, seqs, 2):
             spread = jnp.where(row == s + lane, twice, 0.0)
@@ -782,24 +804,23 @@
                 new_ref[s + t, h] = gamma * state_ref[s + t, h] + added[:, t * dim : (t + 1) * dim]
 
 
-def update(out, key, value, state):
+def update(packed, state):
     seqs, heads, dim = state.shape[:3]
+    width = packed.shape[1] - 2 * heads * dim
     few = min(8, seqs)
     held = pl.BlockSpec((few, heads, dim, dim), lambda j: (j, 0, 0, 0))
-    piece = pl.BlockSpec((few, heads * dim), lambda j: (j, 0))
-    whole = pl.BlockSpec(out.shape, lambda j: (0, 0))
     return pl.pallas_call(
-        functools.partial(update_kernel, heads),
+        update_kernel,
         grid=(seqs // few,),
         out_shape=(
-            jax.ShapeDtypeStruct(out.shape, BF16),
+            jax.ShapeDtypeStruct((seqs, width), BF16),
             jax.ShapeDtypeStruct(state.shape, F32),
         ),
-        in_specs=[whole, piece, piece, held],
-        out_specs=(whole, held),
-        compiler_params=pltpu.CompilerParams(vmem_limit_bytes=60 * 2**20),
+        in_specs=[pl.BlockSpec((few, packed.shape[1]), lambda j: (j, 0)), held],
+        out_specs=(pl.BlockSpec((few, width), lambda j: (j, 0)), held),
+        compiler_params=pltpu.CompilerParams(vmem_limit_bytes=16 * 2**20),
         name="update",
-    )(out, key, value, state)
+    )(packed, state)
 
 
 def on_device(
@@ -830,13 +851,13 @@
     assert w_query.shape[1] % WIDE == 0 and WIDE % dim == 0
     turns = 10000.0 ** (-2.0 * np.arange(dim // 2) / dim)
     freq = jnp.asarray(np.concatenate([turns, turns])[None].astype(np.float32))
-    out, key, value = layer(
+    packed = layer(
         n,
         (inputs, positions, freq, route_ids.T, route_weight.T, norm_mix, norm_ffn, branch_gate,
          head_gain, ret_state, w_query, w_key, w_value, w_gate_in, w_out, exp_gate, exp_up,
          exp_down, dense_gate, dense_up, dense_down),
     )
-    return update(out, key, value, ret_state)
+    return update(packed, ret_state)
 
 
 def solution(mesh):

time: 67.1 us -> 65.5 us (0.976)
  Pallas kernels: 66.3 us -> 63.7 us
  local copies, waits for them, and re-layouts: 0 us -> 0.94 us
    pallas_call x1, Pallas kernels: 5.29 us -> 3.34 us  [update(): pl.pallas_call(update_kernel, grid=(seqs // few,), out_shape=(jax.ShapeDt...]
    unnamed x0 -> x4, local copies, waits for them, and re-layouts: none -> 0.94 us
where the time goes in v4:
time: 65.5 us; the launch traced here: 65.3 us
  Pallas kernels  63.7 us (97%)
  local copies, waits for them, and re-layouts  0.94 us (1%)
  between operations  0.67 us (1%)
    pallas_call x1, Pallas kernels, layer(): pl.pallas_call(functools.partial(layer_kernel, n, heads, dim), out_shape=...  60.4 us
    pallas_call x1, Pallas kernels, update(): pl.pallas_call(update_kernel, grid=(seqs // few,), out_shape=(jax.ShapeDt...  3.34 us

profile of v4, /device:TPU:0, one launch (start us, length us, event | category | flops | bytes accessed | tf_op | source)
XLA Modules:
  0.0 65.3 jit_solution(9970913467550995662)
XLA Ops:
  0.6 0.0 copy-start
  0.6 60.4 %layer.1.packed = f32[16,3584]{1,0:T(8,128)} custom-call(bf16[16,2048]{1,0:T(8,128)(2,1)} %x_hbm.1, s32[16]{0:T(128)} %pos_hbm.1, f32[1,128]{1,0:T(1,128)} %constant.2.clone.freq_hbm, s32[4,16]{1,0:T(4,128)} %bitcast.2, bf16[4,16]{1,0:T(4,128)(2,1)} %bitcast.3, bf16[2048]{0:T(1024)(128)(2,1)} %nmix_hbm.1, bf16[2048]{0:T(1024)(128)(2,1)} %nffn_hbm.1, ...), custom_call_target="tpu_custom_call" | custom-call | tf_op jit(solution)/shard_map/layer/pallas_call | solution.py:713
  61.0 0.0 copy-done
  61.1 0.0 copy-start.1
  61.1 0.9 %copy-done.1 = f32[16,3584]{1,0:T(8,128)S(1)} copy-done((f32[16,3584]{1,0:T(8,128)S(1)}, f32[16,3584]{1,0:T(8,128)}, u32[]{:S(2)}) %copy-start.1) | copy-done | bytes 229400
  62.0 3.3 %update.1 = (bf16[16,2048]{1,0:T(8,128)(2,1)}, f32[16,6,128,128]{3,2,1,0:T(8,128)}) custom-call(f32[16,3584]{1,0:T(8,128)S(1)} %copy-done.1, f32[16,6,128,128]{3,2,1,0:T(8,128)S(1)} %copy-done), custom_call_target="tpu_custom_call" | custom-call | tf_op jit(solution)/shard_map/update/pallas_call | solution.py:812
Async XLA Ops:
  0.6 60.4 %copy-start = (f32[16,6,128,128]{3,2,1,0:T(8,128)S(1)}, f32[16,6,128,128]{3,2,1,0:T(8,128)}, u32[]{:S(2)}) copy-start(f32[16,6,128,128]{3,2,1,0:T(8,128)} %state_ref.1) | copy-start | bytes 18874372
  61.1 0.9 %copy-start.1 = (f32[16,3584]{1,0:T(8,128)S(1)}, f32[16,3584]{1,0:T(8,128)}, u32[]{:S(2)}) copy-start(f32[16,3584]{1,0:T(8,128)} %layer.1.packed) | copy-start | bytes 688132

commit v5 on v4

--- a/solution.py
+++ b/solution.py
@@ -119,6 +119,7 @@
             def _(peer=peer):
                 act(peer)
 
+    order = (lax.rem(INNER + 3 + 2 * INNER - 2 * i, INNER), lax.rem(INNER + 1 - 2 * lax.rem(i, 2), INNER), 2)
     barrier = pltpu.get_barrier_semaphore()
 
     def greet(ep, core):
@@ -302,7 +303,7 @@
         parts[c] = product.astype(BF16).reshape(n, seqs, WIDE)
         scatter(c)
 
-    for k in range(1, INNER):
+    for k in order:
         block_to(k).start()
 
     @pl.when(holder == tp)
@@ -458,7 +459,7 @@
     def _(d):
         on_line(outer - d, lambda peer: along(peer, me).start())
 
-    for k in range(1, INNER):
+    for k in order:
         inside(rblock, k, o, me).start()
     across_cores(rblock, tp, me).start()
 
@@ -471,7 +472,7 @@
     def relay(peer):
         came = peer * INNER + i
         along(peer, came).wait_recv()
-        for j in range(1, INNER):
+        for j in order:
             inside(gathered.at[tp, came], j, peer, came).start()
         across_cores(gathered.at[tp, came], tp, came).start()
 
@@ -617,7 +618,7 @@
         )
 
     def send_group(c, z):
-        for j in range(1, INNER):
+        for j in order:
             in_group(c, z, j, i).start()
 
     for c in range(CHUNKS):

time: 65.5 us -> 65.6 us (level)
  no operation moved by 1% of the time
where the time goes in v5:
time: 65.6 us; the launch traced here: 65.5 us
  Pallas kernels  63.9 us (97%)
  local copies, waits for them, and re-layouts  0.94 us (1%)
  between operations  0.67 us (1%)
    pallas_call x1, Pallas kernels, layer(): pl.pallas_call(functools.partial(layer_kernel, n, heads, dim), out_shape=...  60.5 us
    pallas_call x1, Pallas kernels, update(): pl.pallas_call(update_kernel, grid=(seqs // few,), out_shape=(jax.ShapeDt...  3.34 us

profile of v5, /device:TPU:0, one launch (start us, length us, event | category | flops | bytes accessed | tf_op | source)
XLA Modules:
  0.0 65.5 jit_solution(10770818906442415182)
XLA Ops:
  0.6 0.0 copy-start
  0.6 60.5 %layer.1.packed = f32[16,3584]{1,0:T(8,128)} custom-call(bf16[16,2048]{1,0:T(8,128)(2,1)} %x_hbm.1, s32[16]{0:T(128)} %pos_hbm.1, f32[1,128]{1,0:T(1,128)} %constant.2.clone.freq_hbm, s32[4,16]{1,0:T(4,128)} %bitcast.2, bf16[4,16]{1,0:T(4,128)(2,1)} %bitcast.3, bf16[2048]{0:T(1024)(128)(2,1)} %nmix_hbm.1, bf16[2048]{0:T(1024)(128)(2,1)} %nffn_hbm.1, ...), custom_call_target="tpu_custom_call" | custom-call | tf_op jit(solution)/shard_map/layer/pallas_call | solution.py:714
  61.2 0.0 copy-done
  61.2 0.0 copy-start.1
  61.2 0.9 %copy-done.1 = f32[16,3584]{1,0:T(8,128)S(1)} copy-done((f32[16,3584]{1,0:T(8,128)S(1)}, f32[16,3584]{1,0:T(8,128)}, u32[]{:S(2)}) %copy-start.1) | copy-done | bytes 229400
  62.1 3.3 %update.1 = (bf16[16,2048]{1,0:T(8,128)(2,1)}, f32[16,6,128,128]{3,2,1,0:T(8,128)}) custom-call(f32[16,3584]{1,0:T(8,128)S(1)} %copy-done.1, f32[16,6,128,128]{3,2,1,0:T(8,128)S(1)} %copy-done), custom_call_target="tpu_custom_call" | custom-call | tf_op jit(solution)/shard_map/update/pallas_call | solution.py:813
Async XLA Ops:
  0.6 60.5 %copy-start = (f32[16,6,128,128]{3,2,1,0:T(8,128)S(1)}, f32[16,6,128,128]{3,2,1,0:T(8,128)}, u32[]{:S(2)}) copy-start(f32[16,6,128,128]{3,2,1,0:T(8,128)} %state_ref.1) | copy-start | bytes 18874372
  61.2 0.9 %copy-start.1 = (f32[16,3584]{1,0:T(8,128)S(1)}, f32[16,3584]{1,0:T(8,128)}, u32[]{:S(2)}) copy-start(f32[16,3584]{1,0:T(8,128)} %layer.1.packed) | copy-start | bytes 688132
